TPU v7x, 32 devices: a whole 2x2x4 slice. The times are simulated.
32 devices in a mesh: sp: 8 (over z, y), tp: 4 (over x, core).
Axes of the slice: x: 2, y: 2, z: 4, core: 2. Of those that a mesh axis runs over, the one named last changes fastest.
Arguments:
- out_cotangent: bfloat16 [1024, 2048], P('sp', 'tp'), may hold values from -6 to 6
- expert_input: bfloat16 [1024, 2048], P('sp', 'tp'), may hold values from -6 to 6
- routes: int32 [1024, 2], P('sp'), may hold values from 0 to 7, as said below
- route_weights: float32 [1024, 2], P('sp'), may hold values from 0.2 to 1
- gate_proj: bfloat16 [8, 2048, 3584], P('sp', None, 'tp'), may hold values from -0.125 to 0.125
- up_proj: bfloat16 [8, 2048, 3584], P('sp', None, 'tp'), may hold values from -0.125 to 0.125
- down_proj: bfloat16 [8, 3584, 2048], P('sp', 'tp'), may hold values from -0.09375 to 0.09375
- conv_out: bfloat16 [1024, 2048], P('sp', 'tp'), may hold values from -27 to 27
- conv_mean: float32 [1024], P('sp'), may hold values from -3 to 3
- conv_rstd: float32 [1024], P('sp'), may hold values from 0.25 to 1
- norm_gain: float32 [2048], P('tp'), may hold values from 0.1 to 1.9
- taps: float32 [31, 2048], P(None, 'tp'), may hold values from -1 to 1
- out_proj: bfloat16 [2048, 2048], P(None, 'tp'), may hold values from -0.125 to 0.125
Outputs:
- gate_grad: bfloat16 [8, 2048, 3584], P('sp', None, 'tp')
- up_grad: bfloat16 [8, 2048, 3584], P('sp', None, 'tp')
- down_grad: bfloat16 [8, 3584, 2048], P('sp', 'tp')
- proj_grad: float32 [2048, 2048], P('sp', 'tp')
- stream_grad: bfloat16 [1024, 2048], P('sp', 'tp')
- conv_in_grad: bfloat16 [1024, 2048], P('sp', 'tp')
Inputs may be any that keep to these rules, and one draw needn't show every extreme that they name: `routes`: each row names 2 different experts. In each aligned block of 128 rows (the rows of one device) no expert is named by more than 48 rows, and one expert, the same in every block, is named by exactly 48 rows of every block.
All inputs are finite; a program needn't handle non-finite values.
Results may differ from a plain program's by a relative error of at most 0.02.
Values may be sent and summed in bfloat16 or wider, within the bound.
A program may use at most 128 MiB of HBM per device.

v0:
```python
import functools

import jax
import jax.numpy as jnp
from jax import lax
from jax.experimental import pallas as pl
from jax.experimental.pallas import tpu as pltpu
from jax.sharding import PartitionSpec as P

OUTER_DIMS = (((0,), (0,)), ((), ()))
INNER_DIMS = (((1,), (1,)), ((), ()))
MESH = pl.DeviceIdType.MESH
VMEM = pltpu.VMEM


def flipped(index, bit):
    return index + bit - 2 * bit * ((index // bit) % 2)


def bits_of(count):
    bits, bit = [], 1
    while bit < count:
        bits.append(bit)
        bit *= 2
    return bits


def greet(devices):
    barrier = pltpu.get_barrier_semaphore()
    for device in devices:
        pl.semaphore_signal(barrier, inc=1, device_id=device, device_id_type=MESH)
    pl.semaphore_wait(barrier, len(devices))


def remote(src, dst, send_sem, recv_sem, device):
    return pltpu.make_async_remote_copy(
        src_ref=src, dst_ref=dst, send_sem=send_sem, recv_sem=recv_sem,
        device_id=device, device_id_type=MESH,
    )


def dispatch_kernel(
    experts, parts, rows_send_ref, cot_send_ref, rows_ref, cot_ref,
    out_send, out_recv, hop_send, hop_recv, local_sem,
):
    me, col = lax.axis_index("sp"), lax.axis_index("tp")
    width = rows_send_ref.shape[2]
    bits = bits_of(parts)[::-1]
    greet(
        [(lax.rem(me + k, experts), col) for k in range(1, experts)]
        + [(me, flipped(col, bit)) for bit in bits]
    )
    sends, fulls = (rows_send_ref, cot_send_ref), (rows_ref, cot_ref)

    def place(kind, source, column):
        return fulls[kind].at[source, :, pl.ds(pl.multiple_of(column * width, width), width)]

    def out_copy(kind, peer):
        return remote(
            sends[kind].at[peer], place(kind, me, col), out_send.at[kind, peer],
            out_recv.at[kind, me], (peer, col),
        )

    own = []
    for kind in range(2):
        own.append(
            pltpu.make_async_copy(sends[kind].at[me], place(kind, me, col), local_sem.at[kind])
        )
        own[kind].start()

        def start_out(k, carry, kind=kind):
            out_copy(kind, lax.rem(me + k, experts)).start()
            return carry

        lax.fori_loop(1, experts, start_out, 0)
    for copy in own:
        copy.wait()

    held = [[col]]
    for bit in bits:
        held.append(held[-1] + [flipped(column, bit) for column in held[-1]])
    starts, total = [], 0
    for level in range(len(bits)):
        starts.append(total)
        total += len(held[level])

    def hop(kind, level, slot, column, source):
        index = starts[level] + slot
        return remote(
            place(kind, source, column), place(kind, source, column),
            hop_send.at[kind, index, source], hop_recv.at[kind, index, source],
            (me, flipped(col, bits[level])),
        )

    def hop_arrival(kind, level, slot, source):
        return hop(kind, level, slot, flipped(held[level][slot], bits[level]), source)

    for kind in range(2):

        def advance(k, carry, kind=kind):
            source = lax.rem(me - k + experts, experts)

            @pl.when((k > 0) & (k < experts))
            def _():
                remote(
                    sends[kind].at[source], place(kind, source, col), out_send.at[kind, source],
                    out_recv.at[kind, source], (source, col),
                ).wait_recv()

            @pl.when(k < experts)
            def _():
                for level in range(len(bits)):
                    hop(kind, level, 0, col, source).start()

            for level in range(1, len(bits)):
                late = lax.rem(me - k + level + 2 * experts, experts)

                @pl.when((k >= level) & (k < experts + level))
                def _(level=level, late=late):
                    size = len(held[level - 1])
                    for slot in range(size):
                        hop_arrival(kind, level - 1, slot, late).wait_recv()
                    for later in range(level, len(bits)):
                        for slot in range(size, 2 * size):
                            hop(kind, later, slot, held[level][slot], late).start()

            return carry

        lax.fori_loop(0, experts + len(bits) - 1, advance, 0)

    for kind in range(2):

        def finish(k, carry, kind=kind):
            source = lax.rem(me + k, experts)
            last = len(bits) - 1
            for slot in range(len(held[last])):
                hop_arrival(kind, last, slot, source).wait_recv()
            for level in range(len(bits)):
                for slot in range(len(held[level])):
                    hop(kind, level, slot, held[level][slot], source).wait_send()

            @pl.when(k > 0)
            def _():
                out_copy(kind, source).wait_send()

            return carry

        lax.fori_loop(0, experts, finish, 0)


def dispatch(rows_send, cot_send, experts, parts):
    _, capacity, width = rows_send.shape
    hops = parts - 1
    full = jax.ShapeDtypeStruct((experts, capacity, width * parts), jnp.bfloat16)
    return pl.pallas_call(
        functools.partial(dispatch_kernel, experts, parts),
        out_shape=(full, full),
        in_specs=[pl.BlockSpec(memory_space=VMEM)] * 2,
        out_specs=[pl.BlockSpec(memory_space=VMEM)] * 2,
        scratch_shapes=[pltpu.SemaphoreType.DMA((2, experts))] * 2
        + [pltpu.SemaphoreType.DMA((2, hops, experts))] * 2
        + [pltpu.SemaphoreType.DMA((2,))],
        compiler_params=pltpu.CompilerParams(collective_id=0, has_side_effects=True),
        name="dispatch",
    )(rows_send, cot_send)


def column_of(row, rows):
    return jnp.broadcast_to(row, (128, rows)).T[:, 0:1]


def combine_kernel(
    experts, parts, partial_ref, conv_out_ref, mean_ref, rstd_ref, gain_ref, routed_ref, near_ref,
    *rest,
):
    bits = bits_of(parts)
    levels = len(bits)
    recv_bufs = rest[:levels]
    work, final = rest[levels], rest[levels + 1]
    hop_send, hop_recv, out_send, out_recv, sw_send, sw_recv = rest[levels + 2 :]
    me, col = lax.axis_index("sp"), lax.axis_index("tp")
    width = routed_ref.shape[2]
    greet(
        [(lax.rem(me + k, experts), col) for k in range(1, experts)]
        + [(me, flipped(col, bit)) for bit in bits]
    )
    tokens = conv_out_ref.shape[0]

    kept = [[col]]
    for bit in reversed(bits):
        kept.insert(0, kept[0] + [flipped(column, bit) for column in kept[0]])
    starts, total = [], 0
    for level in range(levels):
        starts.append(total)
        total += len(kept[level + 1])

    def columns(column):
        return pl.ds(pl.multiple_of(column * width, width), width)

    def hop(level, slot, block):
        column = flipped(kept[level + 1][slot], bits[level])
        index = starts[level] + slot
        if level == 0:
            src = partial_ref.at[block, :, columns(column)]
        else:
            src = work.at[level - 1, slot, block]
        return remote(
            src, recv_bufs[level].at[slot, block], hop_send.at[index, block],
            hop_recv.at[index, block], (me, flipped(col, bits[level])),
        )

    def summed(level, slot_column, slot_path, block):
        value = partial_ref[block, :, columns(slot_column)].astype(jnp.float32)
        for stage in range(level):
            value = value + recv_bufs[stage][slot_path[stage], block].astype(jnp.float32)
        return value

    def block_of(k):
        return lax.rem(me + k, experts)

    def start_first(k, carry):
        for slot in range(len(kept[1])):
            hop(0, slot, block_of(k)).start()
        return carry

    lax.fori_loop(1, experts + 1, start_first, 0)

    scaled = (
        (conv_out_ref[...].astype(jnp.float32) - column_of(mean_ref[...], tokens))
        * column_of(rstd_ref[...], tokens)
        * gain_ref[...]
    )
    near_ref[me // 2] = (scaled * jax.nn.sigmoid(scaled)).astype(jnp.bfloat16)

    far_bits = bits_of(experts)[:0:-1]
    sources = [[me]]
    for bit in far_bits:
        sources.append(sources[-1] + [flipped(source, bit) for source in sources[-1]])

    def sw_copy(level, slot, source):
        index = (1 << level) - 1 + slot
        return remote(
            near_ref.at[source // 2], near_ref.at[source // 2], sw_send.at[index],
            sw_recv.at[index], (flipped(me, far_bits[level]), col),
        )

    def sw_start(level):
        for slot, source in enumerate(sources[level]):
            sw_copy(level, slot, source).start()

    def sw_arrive(level):
        for slot, source in enumerate(sources[level]):
            sw_copy(level, slot, flipped(source, far_bits[level])).wait_recv()

    for level in range(1, levels):

        def middle(k, carry, level=level):
            block = block_of(k)
            for slot in range(len(kept[level])):
                hop(level - 1, slot, block).wait_recv()
            size = len(kept[level + 1])
            for slot in range(size):
                value = summed(
                    level, kept[level][size + slot], [size + slot] * level, block
                )
                work[level - 1, slot, block] = value.astype(jnp.bfloat16)
            for slot in range(size):
                hop(level, slot, block).start()
            return carry

        lax.fori_loop(1, experts + 1, middle, 0)

    sw_start(0)

    def out_copy(block):
        return remote(
            final.at[block], routed_ref.at[me], out_send.at[block], out_recv.at[me], (block, col)
        )

    def last(k, carry):
        block = block_of(k)
        hop(levels - 1, 0, block).wait_recv()
        value = summed(levels, col, [0] * levels, block).astype(jnp.bfloat16)

        @pl.when(k < experts)
        def _():
            final[block] = value
            out_copy(block).start()

        @pl.when(k == experts)
        def _():
            routed_ref[me] = value

        return carry

    lax.fori_loop(1, experts + 1, last, 0)
    for level in range(len(far_bits)):
        sw_arrive(level)
        if level + 1 < len(far_bits):
            sw_start(level + 1)

    def finish(k, carry):
        block = block_of(k)
        for level in range(levels):
            for slot in range(len(kept[level + 1])):
                hop(level, slot, block).wait_send()

        @pl.when(k < experts)
        def _():
            out_copy(block).wait_send()
            remote(
                final.at[block], routed_ref.at[block], out_send.at[block],
                out_recv.at[block], (block, col),
            ).wait_recv()

        return carry

    lax.fori_loop(1, experts + 1, finish, 0)
    for level in range(len(far_bits)):
        for slot, source in enumerate(sources[level]):
            sw_copy(level, slot, source).wait_send()


def combine(partial, conv_out, mean, rstd, gain, experts, parts):
    _, capacity, full = partial.shape
    width = full // parts
    levels = len(bits_of(parts))
    hops = parts - 1
    recv = [
        VMEM((parts >> (level + 1), experts, capacity, width), jnp.bfloat16)
        for level in range(levels)
    ]
    return pl.pallas_call(
        functools.partial(combine_kernel, experts, parts),
        out_shape=(
            jax.ShapeDtypeStruct((experts, capacity, width), jnp.bfloat16),
            jax.ShapeDtypeStruct((experts // 2,) + conv_out.shape, jnp.bfloat16),
        ),
        in_specs=[pl.BlockSpec(memory_space=VMEM)] * 5,
        out_specs=[pl.BlockSpec(memory_space=VMEM)] * 2,
        scratch_shapes=recv
        + [
            VMEM((max(levels - 1, 1), max(parts // 4, 1), experts, capacity, width), jnp.bfloat16),
            VMEM((experts, capacity, width), jnp.bfloat16),
            pltpu.SemaphoreType.DMA((hops, experts)),
            pltpu.SemaphoreType.DMA((hops, experts)),
            pltpu.SemaphoreType.DMA((experts,)),
            pltpu.SemaphoreType.DMA((experts,)),
            pltpu.SemaphoreType.DMA((experts // 2,)),
            pltpu.SemaphoreType.DMA((experts // 2,)),
        ],
        compiler_params=pltpu.CompilerParams(collective_id=1, has_side_effects=True),
        name="combine",
    )(partial, conv_out, mean, rstd, gain)


def tail_kernel(
    experts, parts, stream_ref, conv_out_ref, mean_ref, rstd_ref, gain_ref, taps_ref, proj_ref,
    near_ref, conv_ref, proj_grad_ref,
    whole, arrived, far, extended, stats, grads, norms,
    hop_send, hop_recv, out_send, out_recv, stat_send, stat_recv, halo_sem, local_sem, far_sem,
):
    me, col = lax.axis_index("sp"), lax.axis_index("tp")
    width, rows = stream_ref.shape
    full = width * parts
    block = full // experts
    bits = bits_of(parts)[::-1]
    tap_count = taps_ref.shape[0]
    halo = extended.shape[0] - rows
    greet(
        [(lax.rem(me + k, experts), col) for k in range(1, experts)]
        + [(me, lax.rem(col + k, parts)) for k in range(1, parts)]
    )

    far_copy = remote(near_ref, far, far_sem.at[0], far_sem.at[1], (flipped(me, 1), col))
    far_copy.start()

    def part(column):
        return whole.at[pl.ds(pl.multiple_of(column * width, width), width), :]

    own = pltpu.make_async_copy(stream_ref, part(col), local_sem.at[0])
    own.start()
    index, held, copies = 0, [col], []
    for level, bit in enumerate(bits):
        for slot, column in enumerate(held):
            src = stream_ref if column is col else part(column)
            copy = remote(
                src, part(column), hop_send.at[index + slot], hop_recv.at[index + slot],
                (me, flipped(col, bit)),
            )
            copy.start()
            copies.append(copy)
        for slot in range(len(held)):
            column = flipped(held[slot], bit)
            remote(
                part(column), part(column), hop_send.at[index + slot], hop_recv.at[index + slot],
                (me, flipped(col, bit)),
            ).wait_recv()
        index += len(held)
        held = held + [flipped(column, bit) for column in held]
    own.wait()

    def piece(peer):
        return whole.at[pl.ds(pl.multiple_of(peer * block, block), block), :]

    def landing(receiver, source):
        slot = lax.rem(receiver + source, 2) * (experts // 2) + source // 2
        return arrived.at[:, pl.ds(pl.multiple_of(slot * rows, rows), rows)]

    def out_copy(peer):
        return remote(piece(peer), landing(peer, me), out_send.at[peer], out_recv.at[me], (peer, col))

    def start_out(k, carry):
        out_copy(lax.rem(me + k, experts)).start()
        return carry

    lax.fori_loop(1, experts, start_out, 0)
    mine = pltpu.make_async_copy(piece(me), landing(me, me), local_sem.at[1])
    mine.start()

    gain = gain_ref[...]
    rstd = column_of(rstd_ref[...], rows)
    swished_grad = lax.dot_general(
        whole[...], proj_ref[...], OUTER_DIMS, preferred_element_type=jnp.float32
    )
    normed = (conv_out_ref[...].astype(jnp.float32) - column_of(mean_ref[...], rows)) * rstd
    scaled = normed * gain
    sig = jax.nn.sigmoid(scaled)
    scaled_grad = swished_grad * sig * (1.0 + scaled * (1.0 - sig)) * gain
    grads[...] = scaled_grad
    norms[...] = normed
    first = jnp.sum(scaled_grad, axis=1, keepdims=True)
    second = jnp.sum(scaled_grad * normed, axis=1, keepdims=True)
    lane = lax.broadcasted_iota(jnp.int32, (rows, 128), 1)
    both = jnp.where(lane == 0, first, second)
    stats[parts] = both.T[:8]
    stat_copies = []
    for k in range(1, parts):
        copy = remote(
            stats.at[parts], stats.at[k], stat_send.at[k], stat_recv.at[k],
            (me, lax.rem(col + k, parts)),
        )
        copy.start()
        stat_copies.append(copy)
    for copy in stat_copies:
        copy.wait()
    total = stats[parts]
    for k in range(1, parts):
        total = total + stats[k]
    total = total / full
    spread = jnp.concatenate([total] * 16, axis=0).T
    first_mean = spread[:, 0:1]
    second_mean = spread[:, 1:2]
    extended[0:rows, :] = rstd * (grads[...] - first_mean - norms[...] * second_mean)

    def halo_copy(device):
        return remote(
            extended.at[pl.ds(0, halo), :], extended.at[pl.ds(rows, halo), :],
            halo_sem.at[0], halo_sem.at[1], (device, col),
        )

    @pl.when(me > 0)
    def _():
        halo_copy(lax.rem(me + experts - 1, experts)).start()

    @pl.when(me == experts - 1)
    def _():
        extended[rows:, :] = jnp.zeros((halo, width), jnp.float32)

    @pl.when(me < experts - 1)
    def _():
        halo_copy(lax.rem(me + experts - 1, experts)).wait_recv()

    for start in range(0, width, 128):
        cols = pl.ds(start, 128)
        total = jnp.zeros((rows, 128), jnp.float32)
        for offset in range(tap_count):
            total = total + taps_ref[offset : offset + 1, cols] * extended[pl.ds(offset, rows), cols]
        conv_ref[:, cols] = total.astype(jnp.bfloat16)

    def finish(k, carry):
        source = lax.rem(me - k + experts, experts)
        remote(
            piece(source), landing(me, source), out_send.at[source], out_recv.at[source], (source, col)
        ).wait_recv()
        out_copy(source).wait_send()
        return carry

    lax.fori_loop(1, experts, finish, 0)
    mine.wait()
    half = experts // 2 * rows
    proj_grad_ref[...] = jnp.dot(
        arrived[:, :half], near_ref[...].reshape(half, width), preferred_element_type=jnp.float32
    )
    far_copy.wait()
    proj_grad_ref[...] += jnp.dot(
        arrived[:, half:], far[...].reshape(half, width), preferred_element_type=jnp.float32
    )
    for copy in copies:
        copy.wait_send()

    @pl.when(me > 0)
    def _():
        halo_copy(lax.rem(me + experts - 1, experts)).wait_send()


def tail(stream_t, conv_out, mean, rstd, gain, taps, proj, near, experts, parts):
    width, rows = stream_t.shape
    full = width * parts
    block = full // experts
    halo = -(-(taps.shape[0] - 1) // 8) * 8
    return pl.pallas_call(
        functools.partial(tail_kernel, experts, parts),
        out_shape=(
            jax.ShapeDtypeStruct((rows, width), jnp.bfloat16),
            jax.ShapeDtypeStruct((block, width), jnp.float32),
        ),
        in_specs=[pl.BlockSpec(memory_space=VMEM)] * 8,
        out_specs=[pl.BlockSpec(memory_space=VMEM)] * 2,
        scratch_shapes=[
            VMEM((full, rows), jnp.bfloat16),
            VMEM((block, experts * rows), jnp.bfloat16),
            VMEM(near.shape, jnp.bfloat16),
            VMEM((rows + halo, width), jnp.float32),
            VMEM((parts + 1, 8, rows), jnp.float32),
            VMEM((rows, width), jnp.float32),
            VMEM((rows, width), jnp.float32),
            pltpu.SemaphoreType.DMA((parts - 1,)),
            pltpu.SemaphoreType.DMA((parts - 1,)),
            pltpu.SemaphoreType.DMA((experts,)),
            pltpu.SemaphoreType.DMA((experts,)),
            pltpu.SemaphoreType.DMA((parts,)),
            pltpu.SemaphoreType.DMA((parts,)),
            pltpu.SemaphoreType.DMA((2,)),
            pltpu.SemaphoreType.DMA((2,)),
            pltpu.SemaphoreType.DMA((2,)),
        ],
        compiler_params=pltpu.CompilerParams(collective_id=2, has_side_effects=True),
        name="tail",
    )(stream_t, conv_out, mean, rstd, gain, taps, proj, near)


def body(
    out_cotangent,
    expert_input,
    routes,
    route_weights,
    gate_proj,
    up_proj,
    down_proj,
    conv_out,
    conv_mean,
    conv_rstd,
    norm_gain,
    taps,
    out_proj,
):
    tok_rows, local_width = out_cotangent.shape
    experts = lax.axis_size("sp")
    parts = lax.axis_size("tp")
    capacity = 3 * tok_rows // experts
    full_width = local_width * parts
    slots = experts * capacity

    chosen = routes[:, :, None] == jnp.arange(experts, dtype=jnp.int32)[None, None, :]
    named = jnp.any(chosen, axis=1)
    weight = jnp.sum(jnp.where(chosen, route_weights[:, :, None], 0.0), axis=1)
    before = jnp.arange(tok_rows)[None, :] < jnp.arange(tok_rows)[:, None]
    rank = jnp.dot(
        before.astype(jnp.bfloat16), named.astype(jnp.bfloat16), preferred_element_type=jnp.float32
    ).astype(jnp.int32)
    rank = jnp.where(named, rank, -1)
    pick = rank.T[:, None, :] == jnp.arange(capacity, dtype=jnp.int32)[None, :, None]
    slot_weight = jnp.sum(jnp.where(pick, weight.T[:, None, :], 0.0), axis=2)
    pick = pick.astype(jnp.bfloat16).reshape(slots, tok_rows)
    send_rows = jnp.dot(pick, expert_input, preferred_element_type=jnp.float32).astype(jnp.bfloat16)
    send_cot = (
        jnp.dot(pick, out_cotangent, preferred_element_type=jnp.float32)
        * slot_weight.reshape(slots, 1)
    ).astype(jnp.bfloat16)
    arrived_rows, arrived_cot = dispatch(
        send_rows.reshape(experts, capacity, local_width),
        send_cot.reshape(experts, capacity, local_width),
        experts, parts,
    )
    rows_in = arrived_rows.reshape(slots, full_width)
    cot_in = arrived_cot.reshape(slots, full_width)
    mean, rstd, gain = conv_mean[None, :], conv_rstd[None, :], norm_gain[None, :]
    gate_local = gate_proj[0]
    up_local = up_proj[0]
    down_local = down_proj[0]
    gate_pre = jnp.dot(rows_in, gate_local, preferred_element_type=jnp.float32)
    up_pre = jnp.dot(rows_in, up_local, preferred_element_type=jnp.float32)
    gate_sigmoid = jax.nn.sigmoid(gate_pre)
    activation = (gate_pre * gate_sigmoid * up_pre).astype(jnp.bfloat16)
    act_grad = lax.dot_general(cot_in, down_local, INNER_DIMS, preferred_element_type=jnp.float32)
    gate_back = (act_grad * up_pre * gate_sigmoid * (1.0 + gate_pre * (1.0 - gate_sigmoid))).astype(
        jnp.bfloat16
    )
    up_back = (act_grad * gate_pre * gate_sigmoid).astype(jnp.bfloat16)
    down_grad = lax.dot_general(
        activation, cot_in, OUTER_DIMS, preferred_element_type=jnp.float32
    ).astype(jnp.bfloat16)[None]
    gate_grad = lax.dot_general(
        rows_in, gate_back, OUTER_DIMS, preferred_element_type=jnp.float32
    ).astype(jnp.bfloat16)[None]
    up_grad = lax.dot_general(
        rows_in, up_back, OUTER_DIMS, preferred_element_type=jnp.float32
    ).astype(jnp.bfloat16)[None]
    partial_rows = lax.dot_general(
        gate_back, gate_local, INNER_DIMS, preferred_element_type=jnp.float32
    )
    partial_rows = partial_rows + lax.dot_general(
        up_back, up_local, INNER_DIMS, preferred_element_type=jnp.float32
    )
    partial = partial_rows.astype(jnp.bfloat16).reshape(experts, capacity, full_width)
    routed, near = combine(partial, conv_out, mean, rstd, gain, experts, parts)
    routed = routed.reshape(slots, local_width)
    routed_sum = lax.dot_general(pick, routed, OUTER_DIMS, preferred_element_type=jnp.float32)
    stream = (out_cotangent.astype(jnp.float32) + routed_sum).astype(jnp.bfloat16)
    conv_in_grad, proj_grad = tail(
        stream.T, conv_out, mean, rstd, gain, taps, out_proj, near, experts, parts
    )
    return (gate_grad, up_grad, down_grad, proj_grad, stream, conv_in_grad)


def solution(mesh):
    in_specs = (
        P("sp", "tp"),
        P("sp", "tp"),
        P("sp", None),
        P("sp", None),
        P("sp", None, "tp"),
        P("sp", None, "tp"),
        P("sp", "tp", None),
        P("sp", "tp"),
        P("sp"),
        P("sp"),
        P("tp"),
        P(None, "tp"),
        P(None, "tp"),
    )
    out_specs = (
        P("sp", None, "tp"),
        P("sp", None, "tp"),
        P("sp", "tp", None),
        P("sp", "tp"),
        P("sp", "tp"),
        P("sp", "tp"),
    )
    return jax.shard_map(body, mesh=mesh, in_specs=in_specs, out_specs=out_specs, check_vma=False)
```

profile of v0, /device:TPU:0, one launch (start us, length us, event | category | flops | bytes accessed | tf_op | source)
XLA Modules:
  0.0 137.1 jit_solution(16188065015692381339)
XLA Ops:
  0.6 0.7 fusion.18
  1.4 0.1 fusion.15
  1.5 0.7 select_reduce_fusion.1
  2.2 0.1 select_reduce_fusion
  2.7 1.0 copy.24
  3.7 1.9 %fusion.12 = bf16[384,512]{1,0:T(8,128)(2,1)} fusion(pred[384,128]{1,0:T(32,128)(4,1)S(1)} %bitcast_compare_fusion, bf16[128,512]{1,0:T(8,128)(2,1)} %param.13, f32[384]{0:T(512)S(1)} %mul.34), kind=kOutput, calls=%fused_computation.19 | convolution fusion | flops 50724864 | bytes 574976 | tf_op jit(solution)/shard_map/dot_general | solution.py:578
  5.6 1.0 convolution_convert_fusion
  6.6 41.7 %dispatch.1 = (bf16[8,48,2048]{2,1,0:T(8,128)(2,1)}, bf16[8,48,2048]{2,1,0:T(8,128)(2,1)}) custom-call(bf16[8,48,512]{2,1,0:T(8,128)(2,1)} %bitcast.61, bf16[8,48,512]{2,1,0:T(8,128)(2,1)} %bitcast.60), custom_call_target="tpu_custom_call" | custom-call | tf_op jit(solution)/shard_map/dispatch/pallas_call | solution.py:155
  48.4 4.4 %fusion.2 = f32[384,896]{1,0:T(8,128)S(1)} fusion(bf16[384,2048]{1,0:T(8,128)(2,1)} %bitcast.70, bf16[1,2048,896]{2,1,0:T(8,128)(2,1)} %param.17), kind=kOutput, calls=%fused_computation.2 | convolution fusion | flops 1409286144 | bytes 6619136 | tf_op jit(solution)/shard_map/dot_general | solution.py:592
  52.9 1.8 %fusion.6 = f32[384,896]{1,0:T(8,128)S(1)} fusion(bf16[384,2048]{1,0:T(8,128)(2,1)S(1)} %bitcast.71, bf16[1,2048,896]{2,1,0:T(8,128)(2,1)S(1)} %copy-done.6), kind=kOutput, calls=%fused_computation.6 | convolution fusion | flops 1409286144 | bytes 6619136 | tf_op jit(solution)/shard_map/dot_general | solution.py:593
  54.7 0.2 copy-done.4
  54.9 0.5 copy-done.8
  55.4 2.1 %multiply_convert_fusion.1 = (bf16[384,896]{1,0:T(8,128)(2,1)S(1)}, bf16[384,896]{1,0:T(8,128)(2,1)S(1)}) fusion(f32[384,896]{1,0:T(8,128)S(1)} %fusion.2, f32[384,896]{1,0:T(8,128)S(1)} %fusion.6, bf16[384,2048]{1,0:T(8,128)(2,1)S(1)} %bitcast.74, bf16[1,896,2048]{2,1,0:T(8,128)(2,1)S(1)} %copy-done.4), kind=kOutput, calls=%fused_computation.15 | convolution fusion | flops 1413758976 | bytes 9371648 | tf_op jit(solution)/shard_map/dot_general | solution.py:596
  57.5 4.0 %convert_bitcast_fusion = bf16[1,896,2048]{2,1,0:T(8,128)(2,1)} fusion(bf16[384,2048]{1,0:T(8,128)(2,1)S(1)} %bitcast.75, f32[384,896]{1,0:T(8,128)S(1)} %fusion.6, f32[384,896]{1,0:T(8,128)S(1)} %fusion.2), kind=kOutput, calls=%fused_computation.10 | convolution fusion | flops 1413185536 | bytes 7995392 | tf_op jit(solution)/shard_map/dot_general | solution.py:601
  61.5 1.8 %fusion = f32[384,2048]{1,0:T(8,128)S(1)} fusion(bf16[384,896]{1,0:T(8,128)(2,1)S(1)} %get-tuple-element.31, bf16[1,2048,896]{2,1,0:T(8,128)(2,1)S(1)} %copy-done.5), kind=kOutput, calls=%fused_computation | convolution fusion | flops 1409286144 | bytes 7503872 | tf_op jit(solution)/shard_map/dot_general | solution.py:610
  63.4 3.0 %add_convert_fusion = bf16[384,2048]{1,0:T(8,128)(2,1)} fusion(f32[384,2048]{1,0:T(8,128)S(1)} %fusion, bf16[384,896]{1,0:T(8,128)(2,1)S(1)} %get-tuple-element.30, bf16[1,2048,896]{2,1,0:T(8,128)(2,1)S(1)} %copy-done.6), kind=kOutput, calls=%fused_computation.13 | convolution fusion | flops 1410859008 | bytes 9076736 | tf_op jit(solution)/shard_map/dot_general | solution.py:613
  66.3 33.3 %combine.1 = (bf16[8,48,512]{2,1,0:T(8,128)(2,1)}, bf16[4,128,512]{2,1,0:T(8,128)(2,1)}) custom-call(bf16[8,48,2048]{2,1,0:T(8,128)(2,1)} %bitcast.59, bf16[128,512]{1,0:T(8,128)(2,1)} %conv_out_ref.3, f32[1,128]{1,0:T(1,128)} %bitcast.66, f32[1,128]{1,0:T(1,128)} %bitcast.68, f32[1,512]{1,0:T(1,128)} %bitcast.64), custom_call_target="tpu_custom_call" | custom-call | tf_op jit(solution)/shard_map/combine/pallas_call | solution.py:333
  99.6 1.3 fusion.14
  100.9 0.8 copy.26
  101.7 25.7 %tail.1 = (bf16[128,512]{1,0:T(8,128)(2,1)}, f32[256,512]{1,0:T(8,128)}) custom-call(bf16[512,128]{1,0:T(8,128)(2,1)} %bitcast.62, bf16[128,512]{1,0:T(8,128)(2,1)} %conv_out_ref.3, f32[1,128]{1,0:T(1,128)} %bitcast.67, f32[1,128]{1,0:T(1,128)} %bitcast.69, f32[1,512]{1,0:T(1,128)} %bitcast.65, f32[31,512]{1,0:T(8,128)} %taps_ref.1, ...), custom_call_target="tpu_custom_call" | custom-call | tf_op jit(solution)/shard_map/tail/pallas_call | solution.py:512
  127.4 4.1 %convert_bitcast_fusion.1 = bf16[1,2048,896]{2,1,0:T(8,128)(2,1)} fusion(bf16[384,2048]{1,0:T(8,128)(2,1)S(1)} %bitcast.72, bf16[384,896]{1,0:T(8,128)(2,1)S(1)} %get-tuple-element.30), kind=kOutput, calls=%fused_computation.11 | convolution fusion | flops 1411121152 | bytes 5931008 | tf_op jit(solution)/shard_map/dot_general | solution.py:607
  131.5 4.1 %convert_bitcast_fusion.2 = bf16[1,2048,896]{2,1,0:T(8,128)(2,1)} fusion(bf16[384,2048]{1,0:T(8,128)(2,1)S(1)} %bitcast.73, bf16[384,896]{1,0:T(8,128)(2,1)S(1)} %get-tuple-element.31), kind=kOutput, calls=%fused_computation.12 | convolution fusion | flops 1411121152 | bytes 5931008 | tf_op jit(solution)/shard_map/dot_general | solution.py:604
  135.6 0.8 copy.34
  136.4 0.7 copy.35
  (20 shorter events, 0.3 us)
Async XLA Ops:
  0.6 5.0 %copy-start = (bf16[128,512]{1,0:T(8,128)(2,1)S(1)}, bf16[128,512]{1,0:T(8,128)(2,1)}, u32[]{:S(2)}) copy-start(bf16[128,512]{1,0:T(8,128)(2,1)} %param.14) | copy-start | bytes 393220
  48.4 4.5 %copy-start.6 = (bf16[1,2048,896]{2,1,0:T(8,128)(2,1)S(1)}, bf16[1,2048,896]{2,1,0:T(8,128)(2,1)}, u32[]{:S(2)}) copy-start(bf16[1,2048,896]{2,1,0:T(8,128)(2,1)} %param.18) | copy-start | bytes 11010052
  48.4 4.5 %copy-start.7 = (bf16[8,48,2048]{2,1,0:T(8,128)(2,1)S(1)}, bf16[8,48,2048]{2,1,0:T(8,128)(2,1)}, u32[]{:S(2)}) copy-start(bf16[8,48,2048]{2,1,0:T(8,128)(2,1)} %get-tuple-element.12) | copy-start | bytes 4718596
  52.8 2.0 %copy-start.4 = (bf16[1,896,2048]{2,1,0:T(8,128)(2,1)S(1)}, bf16[1,896,2048]{2,1,0:T(8,128)(2,1)}, u32[]{:S(2)}) copy-start(bf16[1,896,2048]{2,1,0:T(8,128)(2,1)} %param.19) | copy-start | bytes 11010052
  52.9 2.5 %copy-start.8 = (bf16[8,48,2048]{2,1,0:T(8,128)(2,1)S(1)}, bf16[8,48,2048]{2,1,0:T(8,128)(2,1)}, u32[]{:S(2)}) copy-start(bf16[8,48,2048]{2,1,0:T(8,128)(2,1)} %get-tuple-element.13) | copy-start | bytes 4718596
  57.5 4.0 %copy-start.5 = (bf16[1,2048,896]{2,1,0:T(8,128)(2,1)S(1)}, bf16[1,2048,896]{2,1,0:T(8,128)(2,1)}, u32[]{:S(2)}) copy-start(bf16[1,2048,896]{2,1,0:T(8,128)(2,1)} %param.17) | copy-start | bytes 11010052
  100.9 0.8 copy-start.1
  131.5 4.1 %copy-start.2 = (f32[256,512]{1,0:T(8,128)S(1)}, f32[256,512]{1,0:T(8,128)}, u32[]{:S(2)}) copy-start(f32[256,512]{1,0:T(8,128)} %get-tuple-element.41) | copy-start | bytes 1572868
  131.5 4.9 %copy-start.3 = (bf16[128,512]{1,0:T(8,128)(2,1)S(1)}, bf16[128,512]{1,0:T(8,128)(2,1)}, u32[]{:S(2)}) copy-start(bf16[128,512]{1,0:T(8,128)(2,1)} %get-tuple-element.43) | copy-start | bytes 393220
where the time goes:
time: 137 us
  Pallas kernels  101 us (74%)
  matrix products  29.7 us (22%)
  local copies, waits for them, and re-layouts  4.16 us (3%)
  other arithmetic  1.7 us (1%)
    pallas_call x1, Pallas kernels, dispatch(): pl.pallas_call(functools.partial(dispatch_kernel, experts, parts), out_sh...  41.7 us
    pallas_call x1, Pallas kernels, combine(): pl.pallas_call(functools.partial(combine_kernel, experts, parts), out_sha...  33.3 us
    pallas_call x1, Pallas kernels, tail(): pl.pallas_call(functools.partial(tail_kernel, experts, parts), out_shape=...  25.7 us
    dot_general x1, matrix products, body(): gate_pre = jnp.dot(rows_in, gate_local, preferred_element_type=jnp.float32)  4.44 us
    dot_general x1, matrix products, body(): lax.dot_general(rows_in, up_back, OUTER_DIMS, preferred_element_type=jnp....  4.11 us
    dot_general x1, matrix products, body(): lax.dot_general(rows_in, gate_back, OUTER_DIMS, preferred_element_type=jn...  4.1 us
    dot_general x1, matrix products, body(): lax.dot_general(activation, cot_in, OUTER_DIMS, preferred_element_type=jn...  4 us
    unnamed x22, local copies, waits for them, and re-layouts  3.99 us

commit v1 on v0

--- a/solution.py
+++ b/solution.py
@@ -15,6 +15,13 @@
 
 def flipped(index, bit):
     return index + bit - 2 * bit * ((index // bit) % 2)
+
+
+def masked(index, mask):
+    for bit in bits_of(mask + 1):
+        if mask & bit:
+            index = flipped(index, bit)
+    return index
 
 
 def bits_of(count):
@@ -67,12 +74,9 @@
             pltpu.make_async_copy(sends[kind].at[me], place(kind, me, col), local_sem.at[kind])
         )
         own[kind].start()
-
-        def start_out(k, carry, kind=kind):
-            out_copy(kind, lax.rem(me + k, experts)).start()
-            return carry
-
-        lax.fori_loop(1, experts, start_out, 0)
+    for kind in range(2):
+        for mask in range(1, experts):
+            out_copy(kind, masked(me, mask)).start()
     for copy in own:
         copy.wait()
 
@@ -95,38 +99,25 @@
     def hop_arrival(kind, level, slot, source):
         return hop(kind, level, slot, flipped(held[level][slot], bits[level]), source)
 
-    for kind in range(2):
-
-        def advance(k, carry, kind=kind):
-            source = lax.rem(me - k + experts, experts)
-
-            @pl.when((k > 0) & (k < experts))
-            def _():
-                remote(
-                    sends[kind].at[source], place(kind, source, col), out_send.at[kind, source],
-                    out_recv.at[kind, source], (source, col),
-                ).wait_recv()
-
-            @pl.when(k < experts)
-            def _():
-                for level in range(len(bits)):
-                    hop(kind, level, 0, col, source).start()
-
-            for level in range(1, len(bits)):
-                late = lax.rem(me - k + level + 2 * experts, experts)
-
-                @pl.when((k >= level) & (k < experts + level))
-                def _(level=level, late=late):
-                    size = len(held[level - 1])
-                    for slot in range(size):
-                        hop_arrival(kind, level - 1, slot, late).wait_recv()
-                    for later in range(level, len(bits)):
-                        for slot in range(size, 2 * size):
-                            hop(kind, later, slot, held[level][slot], late).start()
-
-            return carry
-
-        lax.fori_loop(0, experts + len(bits) - 1, advance, 0)
+    pieces = [(kind, mask) for kind in range(2) for mask in range(experts)]
+    for kind, mask in [(0, 0), (1, 0)] + [piece for piece in pieces if piece[1]]:
+        source = masked(me, mask)
+        if mask:
+            remote(
+                sends[kind].at[source], place(kind, source, col), out_send.at[kind, source],
+                out_recv.at[kind, source], (source, col),
+            ).wait_recv()
+        for level in range(len(bits)):
+            hop(kind, level, 0, col, source).start()
+    for level in range(1, len(bits)):
+        size = len(held[level - 1])
+        for kind, mask in pieces:
+            source = masked(me, mask)
+            for slot in range(size):
+                hop_arrival(kind, level - 1, slot, source).wait_recv()
+            for later in range(level, len(bits)):
+                for slot in range(size, 2 * size):
+                    hop(kind, later, slot, held[level][slot], source).start()
 
     for kind in range(2):
 

time: 137 us -> 125 us (0.912)
  Pallas kernels: 101 us -> 88 us
    pallas_call x1, Pallas kernels: 41.7 us -> 32.3 us  [dispatch(): pl.pallas_call(functools.partial(dispatch_kernel, experts, parts), out_sh...]
    pallas_call x1, Pallas kernels: 33.3 us -> 29.1 us  [combine(): pl.pallas_call(functools.partial(combine_kernel, experts, parts), out_sha...]
where the time goes in v1:
time: 125 us; the launch traced here: 124 us
  Pallas kernels  88 us (70%)
  matrix products  29.7 us (24%)
  local copies, waits for them, and re-layouts  4.16 us (3%)
  other arithmetic  1.7 us (1%)
    pallas_call x1, Pallas kernels, dispatch(): pl.pallas_call(functools.partial(dispatch_kernel, experts, parts), out_sh...  32.3 us
    pallas_call x1, Pallas kernels, combine(): pl.pallas_call(functools.partial(combine_kernel, experts, parts), out_sha...  29.1 us
    pallas_call x1, Pallas kernels, tail(): pl.pallas_call(functools.partial(tail_kernel, experts, parts), out_shape=...  26.6 us
    dot_general x1, matrix products, body(): gate_pre = jnp.dot(rows_in, gate_local, preferred_element_type=jnp.float32)  4.44 us
    dot_general x1, matrix products, body(): lax.dot_general(rows_in, up_back, OUTER_DIMS, preferred_element_type=jnp....  4.11 us
    dot_general x1, matrix products, body(): lax.dot_general(rows_in, gate_back, OUTER_DIMS, preferred_element_type=jn...  4.1 us
    dot_general x1, matrix products, body(): lax.dot_general(activation, cot_in, OUTER_DIMS, preferred_element_type=jn...  4 us
    unnamed x22, local copies, waits for them, and re-layouts  3.99 us

profile of v1, /device:TPU:0, one launch (start us, length us, event | category | flops | bytes accessed | tf_op | source)
XLA Modules:
  0.0 124.3 jit_solution(7924191054450578436)
XLA Ops:
  0.6 0.7 fusion.18
  1.4 0.1 fusion.15
  1.5 0.7 select_reduce_fusion.1
  2.2 0.1 select_reduce_fusion
  2.7 1.0 copy.24
  3.7 1.9 %fusion.12 = bf16[384,512]{1,0:T(8,128)(2,1)} fusion(pred[384,128]{1,0:T(32,128)(4,1)S(1)} %bitcast_compare_fusion, bf16[128,512]{1,0:T(8,128)(2,1)} %param.13, f32[384]{0:T(512)S(1)} %mul.34), kind=kOutput, calls=%fused_computation.19 | convolution fusion | flops 50724864 | bytes 574976 | tf_op jit(solution)/shard_map/dot_general | solution.py:569
  5.6 1.0 convolution_convert_fusion
  6.6 32.3 %dispatch.1 = (bf16[8,48,2048]{2,1,0:T(8,128)(2,1)}, bf16[8,48,2048]{2,1,0:T(8,128)(2,1)}) custom-call(bf16[8,48,512]{2,1,0:T(8,128)(2,1)} %bitcast.61, bf16[8,48,512]{2,1,0:T(8,128)(2,1)} %bitcast.60), custom_call_target="tpu_custom_call" | custom-call | tf_op jit(solution)/shard_map/dispatch/pallas_call | solution.py:146
  38.9 4.4 %fusion.2 = f32[384,896]{1,0:T(8,128)S(1)} fusion(bf16[384,2048]{1,0:T(8,128)(2,1)} %bitcast.70, bf16[1,2048,896]{2,1,0:T(8,128)(2,1)} %param.17), kind=kOutput, calls=%fused_computation.2 | convolution fusion | flops 1409286144 | bytes 6619136 | tf_op jit(solution)/shard_map/dot_general | solution.py:583
  43.4 1.8 %fusion.6 = f32[384,896]{1,0:T(8,128)S(1)} fusion(bf16[384,2048]{1,0:T(8,128)(2,1)S(1)} %bitcast.71, bf16[1,2048,896]{2,1,0:T(8,128)(2,1)S(1)} %copy-done.6), kind=kOutput, calls=%fused_computation.6 | convolution fusion | flops 1409286144 | bytes 6619136 | tf_op jit(solution)/shard_map/dot_general | solution.py:584
  45.2 0.2 copy-done.4
  45.5 0.5 copy-done.8
  45.9 2.1 %multiply_convert_fusion.1 = (bf16[384,896]{1,0:T(8,128)(2,1)S(1)}, bf16[384,896]{1,0:T(8,128)(2,1)S(1)}) fusion(f32[384,896]{1,0:T(8,128)S(1)} %fusion.2, f32[384,896]{1,0:T(8,128)S(1)} %fusion.6, bf16[384,2048]{1,0:T(8,128)(2,1)S(1)} %bitcast.74, bf16[1,896,2048]{2,1,0:T(8,128)(2,1)S(1)} %copy-done.4), kind=kOutput, calls=%fused_computation.15 | convolution fusion | flops 1413758976 | bytes 9371648 | tf_op jit(solution)/shard_map/dot_general | solution.py:587
  48.1 4.0 %convert_bitcast_fusion = bf16[1,896,2048]{2,1,0:T(8,128)(2,1)} fusion(bf16[384,2048]{1,0:T(8,128)(2,1)S(1)} %bitcast.75, f32[384,896]{1,0:T(8,128)S(1)} %fusion.6, f32[384,896]{1,0:T(8,128)S(1)} %fusion.2), kind=kOutput, calls=%fused_computation.10 | convolution fusion | flops 1413185536 | bytes 7995392 | tf_op jit(solution)/shard_map/dot_general | solution.py:592
  52.1 1.8 %fusion = f32[384,2048]{1,0:T(8,128)S(1)} fusion(bf16[384,896]{1,0:T(8,128)(2,1)S(1)} %get-tuple-element.31, bf16[1,2048,896]{2,1,0:T(8,128)(2,1)S(1)} %copy-done.5), kind=kOutput, calls=%fused_computation | convolution fusion | flops 1409286144 | bytes 7503872 | tf_op jit(solution)/shard_map/dot_general | solution.py:601
  53.9 3.0 %add_convert_fusion = bf16[384,2048]{1,0:T(8,128)(2,1)} fusion(f32[384,2048]{1,0:T(8,128)S(1)} %fusion, bf16[384,896]{1,0:T(8,128)(2,1)S(1)} %get-tuple-element.30, bf16[1,2048,896]{2,1,0:T(8,128)(2,1)S(1)} %copy-done.6), kind=kOutput, calls=%fused_computation.13 | convolution fusion | flops 1410859008 | bytes 9076736 | tf_op jit(solution)/shard_map/dot_general | solution.py:604
  56.9 29.1 %combine.1 = (bf16[8,48,512]{2,1,0:T(8,128)(2,1)}, bf16[4,128,512]{2,1,0:T(8,128)(2,1)}) custom-call(bf16[8,48,2048]{2,1,0:T(8,128)(2,1)} %bitcast.59, bf16[128,512]{1,0:T(8,128)(2,1)} %conv_out_ref.3, f32[1,128]{1,0:T(1,128)} %bitcast.66, f32[1,128]{1,0:T(1,128)} %bitcast.68, f32[1,512]{1,0:T(1,128)} %bitcast.64), custom_call_target="tpu_custom_call" | custom-call | tf_op jit(solution)/shard_map/combine/pallas_call | solution.py:324
  86.0 1.3 %fusion.14 = bf16[128,512]{0,1:T(8,128)(2,1)S(1)} fusion(bf16[8,48,512]{2,1,0:T(8,128)(2,1)} %get-tuple-element.14, bf16[128,512]{0,1:T(8,128)(2,1)S(1)} %copy.24, s32[8,128]{1,0:T(8,128)S(1)} %fusion.15), kind=kOutput, calls=%fused_computation.23 | convolution fusion | flops 50577408 | bytes 659456 | tf_op jit(solution)/shard_map/dot_general | solution.py:610
  87.3 0.8 copy.26
  88.1 26.6 %tail.1 = (bf16[128,512]{1,0:T(8,128)(2,1)}, f32[256,512]{1,0:T(8,128)}) custom-call(bf16[512,128]{1,0:T(8,128)(2,1)} %bitcast.62, bf16[128,512]{1,0:T(8,128)(2,1)} %conv_out_ref.3, f32[1,128]{1,0:T(1,128)} %bitcast.67, f32[1,128]{1,0:T(1,128)} %bitcast.69, f32[1,512]{1,0:T(1,128)} %bitcast.65, f32[31,512]{1,0:T(8,128)} %taps_ref.1, ...), custom_call_target="tpu_custom_call" | custom-call | tf_op jit(solution)/shard_map/tail/pallas_call | solution.py:503
  114.7 4.1 %convert_bitcast_fusion.1 = bf16[1,2048,896]{2,1,0:T(8,128)(2,1)} fusion(bf16[384,2048]{1,0:T(8,128)(2,1)S(1)} %bitcast.72, bf16[384,896]{1,0:T(8,128)(2,1)S(1)} %get-tuple-element.30), kind=kOutput, calls=%fused_computation.11 | convolution fusion | flops 1411121152 | bytes 5931008 | tf_op jit(solution)/shard_map/dot_general | solution.py:598
  118.8 4.1 %convert_bitcast_fusion.2 = bf16[1,2048,896]{2,1,0:T(8,128)(2,1)} fusion(bf16[384,2048]{1,0:T(8,128)(2,1)S(1)} %bitcast.73, bf16[384,896]{1,0:T(8,128)(2,1)S(1)} %get-tuple-element.31), kind=kOutput, calls=%fused_computation.12 | convolution fusion | flops 1411121152 | bytes 5931008 | tf_op jit(solution)/shard_map/dot_general | solution.py:595
  122.9 0.8 copy.34
  123.7 0.7 copy.35
  (20 shorter events, 0.3 us)
Async XLA Ops:
  0.6 5.0 %copy-start = (bf16[128,512]{1,0:T(8,128)(2,1)S(1)}, bf16[128,512]{1,0:T(8,128)(2,1)}, u32[]{:S(2)}) copy-start(bf16[128,512]{1,0:T(8,128)(2,1)} %param.14) | copy-start | bytes 393220
  38.9 4.5 %copy-start.6 = (bf16[1,2048,896]{2,1,0:T(8,128)(2,1)S(1)}, bf16[1,2048,896]{2,1,0:T(8,128)(2,1)}, u32[]{:S(2)}) copy-start(bf16[1,2048,896]{2,1,0:T(8,128)(2,1)} %param.18) | copy-start | bytes 11010052
  38.9 4.5 %copy-start.7 = (bf16[8,48,2048]{2,1,0:T(8,128)(2,1)S(1)}, bf16[8,48,2048]{2,1,0:T(8,128)(2,1)}, u32[]{:S(2)}) copy-start(bf16[8,48,2048]{2,1,0:T(8,128)(2,1)} %get-tuple-element.12) | copy-start | bytes 4718596
  43.4 2.0 %copy-start.4 = (bf16[1,896,2048]{2,1,0:T(8,128)(2,1)S(1)}, bf16[1,896,2048]{2,1,0:T(8,128)(2,1)}, u32[]{:S(2)}) copy-start(bf16[1,896,2048]{2,1,0:T(8,128)(2,1)} %param.19) | copy-start | bytes 11010052
  43.4 2.5 %copy-start.8 = (bf16[8,48,2048]{2,1,0:T(8,128)(2,1)S(1)}, bf16[8,48,2048]{2,1,0:T(8,128)(2,1)}, u32[]{:S(2)}) copy-start(bf16[8,48,2048]{2,1,0:T(8,128)(2,1)} %get-tuple-element.13) | copy-start | bytes 4718596
  48.1 4.0 %copy-start.5 = (bf16[1,2048,896]{2,1,0:T(8,128)(2,1)S(1)}, bf16[1,2048,896]{2,1,0:T(8,128)(2,1)}, u32[]{:S(2)}) copy-start(bf16[1,2048,896]{2,1,0:T(8,128)(2,1)} %param.17) | copy-start | bytes 11010052
  87.3 0.8 copy-start.1
  118.8 4.1 %copy-start.2 = (f32[256,512]{1,0:T(8,128)S(1)}, f32[256,512]{1,0:T(8,128)}, u32[]{:S(2)}) copy-start(f32[256,512]{1,0:T(8,128)} %get-tuple-element.41) | copy-start | bytes 1572868
  118.8 4.9 %copy-start.3 = (bf16[128,512]{1,0:T(8,128)(2,1)S(1)}, bf16[128,512]{1,0:T(8,128)(2,1)}, u32[]{:S(2)}) copy-start(bf16[128,512]{1,0:T(8,128)(2,1)} %get-tuple-element.43) | copy-start | bytes 393220

commit v2 on v1

--- a/solution.py
+++ b/solution.py
@@ -46,37 +46,65 @@
     )
 
 
-def dispatch_kernel(
-    experts, parts, rows_send_ref, cot_send_ref, rows_ref, cot_ref,
-    out_send, out_recv, hop_send, hop_recv, local_sem,
+def column_of(row, rows):
+    return jnp.broadcast_to(row, (128, rows)).T[:, 0:1]
+
+
+def ladder(experts):
+    half = experts // 2
+    return list(range(half, experts)) + list(range(1, half))
+
+
+def front_kernel(
+    experts, parts, rows_send_ref, cot_send_ref, pick_ref, cotangent_ref, conv_out_ref, mean_ref,
+    rstd_ref, gain_ref, gate_hbm, up_hbm, down_hbm,
+    rows_out, cot_out, act_out, gate_out, up_out, stream_ref, stream_t_ref, near_ref,
+    gate, up, down, full, gate_pre, up_pre, act_grad, backs, partial, first_recv, recv, work, final,
+    routed, out_send, out_recv, hop_send, hop_recv, first_sems, back_send, back_recv, home_send,
+    home_recv, sw_send, sw_recv, weight_sem, save_sem, own_sem,
 ):
     me, col = lax.axis_index("sp"), lax.axis_index("tp")
-    width = rows_send_ref.shape[2]
-    bits = bits_of(parts)[::-1]
+    width = rows_send_ref.shape[1]
+    capacity = rows_send_ref.shape[0] // experts
+    hidden = gate.shape[1]
+    tokens = conv_out_ref.shape[0]
+    up_bits = bits_of(parts)
+    bits = up_bits[::-1]
+    levels = len(bits)
+    loads = []
+    for index, (src, dst) in enumerate(((gate_hbm, gate), (up_hbm, up), (down_hbm, down))):
+        loads.append(pltpu.make_async_copy(src.at[0], dst, weight_sem.at[index]))
+        loads[-1].start()
     greet(
         [(lax.rem(me + k, experts), col) for k in range(1, experts)]
         + [(me, flipped(col, bit)) for bit in bits]
     )
-    sends, fulls = (rows_send_ref, cot_send_ref), (rows_ref, cot_ref)
+    sends = (rows_send_ref, cot_send_ref)
+
+    def block_rows(source):
+        return pl.ds(pl.multiple_of(source * capacity, capacity), capacity)
 
     def place(kind, source, column):
-        return fulls[kind].at[source, :, pl.ds(pl.multiple_of(column * width, width), width)]
-
-    def out_copy(kind, peer):
+        return full.at[kind, column, block_rows(source), :]
+
+    def out_copy(kind, peer, owner):
         return remote(
-            sends[kind].at[peer], place(kind, me, col), out_send.at[kind, peer],
-            out_recv.at[kind, me], (peer, col),
-        )
-
+            sends[kind].at[block_rows(peer), :], place(kind, owner, col), out_send.at[kind, peer],
+            out_recv.at[kind, owner], (peer, col),
+        )
+
+    for kind in range(2):
+        for mask in range(1, experts):
+            peer = masked(me, mask)
+            out_copy(kind, peer, me).start()
     own = []
     for kind in range(2):
         own.append(
-            pltpu.make_async_copy(sends[kind].at[me], place(kind, me, col), local_sem.at[kind])
+            pltpu.make_async_copy(
+                sends[kind].at[block_rows(me), :], place(kind, me, col), own_sem.at[kind]
+            )
         )
         own[kind].start()
-    for kind in range(2):
-        for mask in range(1, experts):
-            out_copy(kind, masked(me, mask)).start()
     for copy in own:
         copy.wait()
 
@@ -84,7 +112,7 @@
     for bit in bits:
         held.append(held[-1] + [flipped(column, bit) for column in held[-1]])
     starts, total = [], 0
-    for level in range(len(bits)):
+    for level in range(levels):
         starts.append(total)
         total += len(held[level])
 
@@ -99,122 +127,37 @@
     def hop_arrival(kind, level, slot, source):
         return hop(kind, level, slot, flipped(held[level][slot], bits[level]), source)
 
-    pieces = [(kind, mask) for kind in range(2) for mask in range(experts)]
-    for kind, mask in [(0, 0), (1, 0)] + [piece for piece in pieces if piece[1]]:
-        source = masked(me, mask)
-        if mask:
-            remote(
-                sends[kind].at[source], place(kind, source, col), out_send.at[kind, source],
-                out_recv.at[kind, source], (source, col),
-            ).wait_recv()
-        for level in range(len(bits)):
+    def first_hops(kind, source):
+        for level in range(levels):
             hop(kind, level, 0, col, source).start()
-    for level in range(1, len(bits)):
+
+    def arrive(kind):
+        for mask in range(1, experts):
+            source = masked(me, mask)
+            out_copy(kind, source, source).wait_recv()
+            first_hops(kind, source)
+
+    def pass_on(kind, masks, level):
         size = len(held[level - 1])
-        for kind, mask in pieces:
+        for mask in masks:
             source = masked(me, mask)
             for slot in range(size):
                 hop_arrival(kind, level - 1, slot, source).wait_recv()
-            for later in range(level, len(bits)):
+            for later in range(level, levels):
                 for slot in range(size, 2 * size):
                     hop(kind, later, slot, held[level][slot], source).start()
 
+    def collect(kind):
+        def step(k, carry):
+            source = lax.rem(me + k, experts)
+            for slot in range(len(held[levels - 1])):
+                hop_arrival(kind, levels - 1, slot, source).wait_recv()
+            return carry
+
+        lax.fori_loop(0, experts, step, 0)
+
     for kind in range(2):
-
-        def finish(k, carry, kind=kind):
-            source = lax.rem(me + k, experts)
-            last = len(bits) - 1
-            for slot in range(len(held[last])):
-                hop_arrival(kind, last, slot, source).wait_recv()
-            for level in range(len(bits)):
-                for slot in range(len(held[level])):
-                    hop(kind, level, slot, held[level][slot], source).wait_send()
-
-            @pl.when(k > 0)
-            def _():
-                out_copy(kind, source).wait_send()
-
-            return carry
-
-        lax.fori_loop(0, experts, finish, 0)
-
-
-def dispatch(rows_send, cot_send, experts, parts):
-    _, capacity, width = rows_send.shape
-    hops = parts - 1
-    full = jax.ShapeDtypeStruct((experts, capacity, width * parts), jnp.bfloat16)
-    return pl.pallas_call(
-        functools.partial(dispatch_kernel, experts, parts),
-        out_shape=(full, full),
-        in_specs=[pl.BlockSpec(memory_space=VMEM)] * 2,
-        out_specs=[pl.BlockSpec(memory_space=VMEM)] * 2,
-        scratch_shapes=[pltpu.SemaphoreType.DMA((2, experts))] * 2
-        + [pltpu.SemaphoreType.DMA((2, hops, experts))] * 2
-        + [pltpu.SemaphoreType.DMA((2,))],
-        compiler_params=pltpu.CompilerParams(collective_id=0, has_side_effects=True),
-        name="dispatch",
-    )(rows_send, cot_send)
-
-
-def column_of(row, rows):
-    return jnp.broadcast_to(row, (128, rows)).T[:, 0:1]
-
-
-def combine_kernel(
-    experts, parts, partial_ref, conv_out_ref, mean_ref, rstd_ref, gain_ref, routed_ref, near_ref,
-    *rest,
-):
-    bits = bits_of(parts)
-    levels = len(bits)
-    recv_bufs = rest[:levels]
-    work, final = rest[levels], rest[levels + 1]
-    hop_send, hop_recv, out_send, out_recv, sw_send, sw_recv = rest[levels + 2 :]
-    me, col = lax.axis_index("sp"), lax.axis_index("tp")
-    width = routed_ref.shape[2]
-    greet(
-        [(lax.rem(me + k, experts), col) for k in range(1, experts)]
-        + [(me, flipped(col, bit)) for bit in bits]
-    )
-    tokens = conv_out_ref.shape[0]
-
-    kept = [[col]]
-    for bit in reversed(bits):
-        kept.insert(0, kept[0] + [flipped(column, bit) for column in kept[0]])
-    starts, total = [], 0
-    for level in range(levels):
-        starts.append(total)
-        total += len(kept[level + 1])
-
-    def columns(column):
-        return pl.ds(pl.multiple_of(column * width, width), width)
-
-    def hop(level, slot, block):
-        column = flipped(kept[level + 1][slot], bits[level])
-        index = starts[level] + slot
-        if level == 0:
-            src = partial_ref.at[block, :, columns(column)]
-        else:
-            src = work.at[level - 1, slot, block]
-        return remote(
-            src, recv_bufs[level].at[slot, block], hop_send.at[index, block],
-            hop_recv.at[index, block], (me, flipped(col, bits[level])),
-        )
-
-    def summed(level, slot_column, slot_path, block):
-        value = partial_ref[block, :, columns(slot_column)].astype(jnp.float32)
-        for stage in range(level):
-            value = value + recv_bufs[stage][slot_path[stage], block].astype(jnp.float32)
-        return value
-
-    def block_of(k):
-        return lax.rem(me + k, experts)
-
-    def start_first(k, carry):
-        for slot in range(len(kept[1])):
-            hop(0, slot, block_of(k)).start()
-        return carry
-
-    lax.fori_loop(1, experts + 1, start_first, 0)
+        first_hops(kind, me)
 
     scaled = (
         (conv_out_ref[...].astype(jnp.float32) - column_of(mean_ref[...], tokens))
@@ -243,106 +186,280 @@
         for slot, source in enumerate(sources[level]):
             sw_copy(level, slot, flipped(source, far_bits[level])).wait_recv()
 
+    arrive(0)
+    arrive(1)
+    sw_start(0)
+    masks = list(range(experts))
     for level in range(1, levels):
-
-        def middle(k, carry, level=level):
-            block = block_of(k)
-            for slot in range(len(kept[level])):
-                hop(level - 1, slot, block).wait_recv()
-            size = len(kept[level + 1])
+        pass_on(0, masks, level)
+    collect(0)
+
+    def tiles(step):
+        whole = hidden // 256
+
+        def one(j, carry):
+            step(pl.ds(pl.multiple_of(j * 256, 256), 256), 256)
+            return carry
+
+        lax.fori_loop(0, whole, one, 0)
+        if hidden % 256:
+            step(pl.ds(whole * 256, hidden % 256), hidden % 256)
+
+    def joined(kind):
+        return jnp.concatenate([full[kind, part] for part in range(parts)], axis=1)
+
+    loads[0].wait()
+    loads[1].wait()
+
+    def pre(cols, size):
+        rows = joined(0)
+        gate_pre[:, cols] = jnp.dot(rows, gate[:, cols], preferred_element_type=jnp.float32)
+        up_pre[:, cols] = jnp.dot(rows, up[:, cols], preferred_element_type=jnp.float32)
+
+    tiles(pre)
+    for level in range(1, levels):
+        pass_on(1, masks, level)
+    collect(1)
+    loads[2].wait()
+
+    def back(cols, size):
+        act_grad[:, 0:size] = lax.dot_general(
+            joined(1), down[cols, :], INNER_DIMS, preferred_element_type=jnp.float32
+        )
+
+        def chunk(k, carry):
+            rows = block_rows(k)
+            gates, ups, grad = gate_pre[rows, cols], up_pre[rows, cols], act_grad[rows, 0:size]
+            sig = jax.nn.sigmoid(gates)
+            silu = gates * sig
+            backs[0, rows, cols] = (silu * ups).astype(jnp.bfloat16)
+            backs[1, rows, cols] = (grad * ups * sig * (1.0 + gates * (1.0 - sig))).astype(
+                jnp.bfloat16
+            )
+            backs[2, rows, cols] = (grad * silu).astype(jnp.bfloat16)
+            return carry
+
+        lax.fori_loop(0, experts, chunk, 0)
+
+    tiles(back)
+    saves = [
+        pltpu.make_async_copy(full.at[0], rows_out, save_sem.at[0]),
+        pltpu.make_async_copy(full.at[1], cot_out, save_sem.at[1]),
+        pltpu.make_async_copy(backs.at[0], act_out, save_sem.at[2]),
+        pltpu.make_async_copy(backs.at[1], gate_out, save_sem.at[3]),
+        pltpu.make_async_copy(backs.at[2], up_out, save_sem.at[4]),
+    ]
+
+    kept = [[col]]
+    for bit in bits:
+        kept.insert(0, kept[0] + [flipped(column, bit) for column in kept[0]])
+    order = ladder(experts) + [0]
+
+    def first_copy(slot):
+        return remote(
+            partial.at[flipped(kept[1][slot], up_bits[0])], first_recv.at[slot],
+            first_sems.at[0, slot], first_sems.at[1, slot], (me, flipped(col, up_bits[0])),
+        )
+
+    def fill(column):
+        rows = pl.ds(pl.multiple_of(column * width, width), width)
+        value = lax.dot_general(
+            backs[1], gate[rows, :], INNER_DIMS, preferred_element_type=jnp.float32
+        ) + lax.dot_general(
+            backs[2], up[rows, :], INNER_DIMS, preferred_element_type=jnp.float32
+        )
+        partial[column] = value.astype(jnp.bfloat16)
+
+    back_starts, total = [0], 0
+    for level in range(1, levels):
+        back_starts.append(total)
+        total += len(kept[level + 1])
+
+    def back_copy(level, slot, block):
+        index = back_starts[level] + slot
+        return remote(
+            work.at[index, block_rows(block), :], recv.at[index, block_rows(block), :],
+            back_send.at[index, block], back_recv.at[index, block],
+            (me, flipped(col, up_bits[level])),
+        )
+
+    def summed(level, slot, block):
+        rows = block_rows(block)
+        value = partial[kept[level][slot], rows, :].astype(jnp.float32)
+        value = value + first_recv[slot, rows, :].astype(jnp.float32)
+        for stage in range(1, level):
+            value = value + recv[back_starts[stage] + slot, rows, :].astype(jnp.float32)
+        return value.astype(jnp.bfloat16)
+
+    for slot in reversed(range(len(kept[1]))):
+        fill(flipped(kept[1][slot], up_bits[0]))
+        first_copy(slot).start()
+        fill(kept[1][slot])
+        first_copy(slot).wait_recv()
+        size = len(kept[2]) if levels > 1 else 0
+        if levels > 1 and slot >= size:
+            for mask in order:
+                block = masked(me, mask)
+                work[back_starts[1] + slot - size, block_rows(block), :] = summed(1, slot, block)
+                back_copy(1, slot - size, block).start()
+    for copy in saves:
+        copy.start()
+    for level in range(2, levels):
+        size = len(kept[level + 1])
+        for mask in order:
+            block = masked(me, mask)
+            for slot in range(2 * size):
+                back_copy(level - 1, slot, block).wait_recv()
             for slot in range(size):
-                value = summed(
-                    level, kept[level][size + slot], [size + slot] * level, block
+                work[back_starts[level] + slot, block_rows(block), :] = summed(
+                    level, size + slot, block
                 )
-                work[level - 1, slot, block] = value.astype(jnp.bfloat16)
-            for slot in range(size):
-                hop(level, slot, block).start()
-            return carry
-
-        lax.fori_loop(1, experts + 1, middle, 0)
-
-    sw_start(0)
-
-    def out_copy(block):
+                back_copy(level, slot, block).start()
+
+    def home_copy(block, owner):
         return remote(
-            final.at[block], routed_ref.at[me], out_send.at[block], out_recv.at[me], (block, col)
-        )
-
-    def last(k, carry):
-        block = block_of(k)
-        hop(levels - 1, 0, block).wait_recv()
-        value = summed(levels, col, [0] * levels, block).astype(jnp.bfloat16)
-
-        @pl.when(k < experts)
-        def _():
-            final[block] = value
-            out_copy(block).start()
-
-        @pl.when(k == experts)
-        def _():
-            routed_ref[me] = value
-
-        return carry
-
-    lax.fori_loop(1, experts + 1, last, 0)
+            final.at[block_rows(block), :], routed.at[block_rows(owner), :],
+            home_send.at[block], home_recv.at[owner], (block, col),
+        )
+
+    for mask in order:
+        block = masked(me, mask)
+        if levels > 1:
+            back_copy(levels - 1, 0, block).wait_recv()
+        value = summed(levels, 0, block)
+        if mask:
+            final[block_rows(block), :] = value
+            home_copy(block, me).start()
+        else:
+            routed[block_rows(block), :] = value
     for level in range(len(far_bits)):
         sw_arrive(level)
         if level + 1 < len(far_bits):
             sw_start(level + 1)
+    for mask in order[:-1]:
+        source = masked(me, mask)
+        home_copy(source, source).wait_recv()
+    stream = cotangent_ref[...].astype(jnp.float32) + jnp.dot(
+        pick_ref[...], routed[...], preferred_element_type=jnp.float32
+    )
+    stream_ref[...] = stream.astype(jnp.bfloat16)
+    stream_t_ref[...] = stream.T.astype(jnp.bfloat16)
 
     def finish(k, carry):
-        block = block_of(k)
-        for level in range(levels):
+        source = lax.rem(me + k, experts)
+        for kind in range(2):
+            for level in range(levels):
+                for slot in range(len(held[level])):
+                    hop(kind, level, slot, held[level][slot], source).wait_send()
+        for level in range(1, levels):
             for slot in range(len(kept[level + 1])):
-                hop(level, slot, block).wait_send()
-
-        @pl.when(k < experts)
+                back_copy(level, slot, source).wait_send()
+
+        @pl.when(k > 0)
         def _():
-            out_copy(block).wait_send()
-            remote(
-                final.at[block], routed_ref.at[block], out_send.at[block],
-                out_recv.at[block], (block, col),
-            ).wait_recv()
+            for kind in range(2):
+                out_copy(kind, source, me).wait_send()
+            home_copy(source, me).wait_send()
 
         return carry
 
-    lax.fori_loop(1, experts + 1, finish, 0)
+    lax.fori_loop(0, experts, finish, 0)
+    for slot in range(len(kept[1])):
+        first_copy(slot).wait_send()
     for level in range(len(far_bits)):
         for slot, source in enumerate(sources[level]):
             sw_copy(level, slot, source).wait_send()
-
-
-def combine(partial, conv_out, mean, rstd, gain, experts, parts):
-    _, capacity, full = partial.shape
-    width = full // parts
-    levels = len(bits_of(parts))
+    for copy in saves:
+        copy.wait()
+
+
+def front(
+    rows_send, cot_send, pick_t, cotangent, conv_out, mean, rstd, gain, gate, up, down, experts, parts
+):
+    slots, width = rows_send.shape
+    full_width, hidden = gate.shape[1:]
+    tokens = conv_out.shape[0]
     hops = parts - 1
-    recv = [
-        VMEM((parts >> (level + 1), experts, capacity, width), jnp.bfloat16)
-        for level in range(levels)
-    ]
+    extra = max(parts // 2 - 1, 1)
+    bf16, dma = jnp.bfloat16, pltpu.SemaphoreType.DMA
+    rows_all = jax.ShapeDtypeStruct((parts, slots, width), bf16)
+    acts = jax.ShapeDtypeStruct((slots, hidden), bf16)
     return pl.pallas_call(
-        functools.partial(combine_kernel, experts, parts),
+        functools.partial(front_kernel, experts, parts),
         out_shape=(
-            jax.ShapeDtypeStruct((experts, capacity, width), jnp.bfloat16),
-            jax.ShapeDtypeStruct((experts // 2,) + conv_out.shape, jnp.bfloat16),
+            rows_all, rows_all, acts, acts, acts,
+            jax.ShapeDtypeStruct((tokens, width), bf16),
+            jax.ShapeDtypeStruct((width, tokens), bf16),
+            jax.ShapeDtypeStruct((experts // 2, tokens, width), bf16),
         ),
-        in_specs=[pl.BlockSpec(memory_space=VMEM)] * 5,
-        out_specs=[pl.BlockSpec(memory_space=VMEM)] * 2,
-        scratch_shapes=recv
-        + [
-            VMEM((max(levels - 1, 1), max(parts // 4, 1), experts, capacity, width), jnp.bfloat16),
-            VMEM((experts, capacity, width), jnp.bfloat16),
-            pltpu.SemaphoreType.DMA((hops, experts)),
-            pltpu.SemaphoreType.DMA((hops, experts)),
-            pltpu.SemaphoreType.DMA((experts,)),
-            pltpu.SemaphoreType.DMA((experts,)),
-            pltpu.SemaphoreType.DMA((experts // 2,)),
-            pltpu.SemaphoreType.DMA((experts // 2,)),
+        in_specs=[pl.BlockSpec(memory_space=VMEM)] * 8 + [pl.BlockSpec(memory_space=pl.ANY)] * 3,
+        out_specs=[pl.BlockSpec(memory_space=pl.ANY)] * 5
+        + [pl.BlockSpec(memory_space=VMEM)] * 3,
+        scratch_shapes=[
+            VMEM((full_width, hidden), bf16),
+            VMEM((full_width, hidden), bf16),
+            VMEM((hidden, full_width), bf16),
+            VMEM((2, parts, slots, width), bf16),
+            VMEM((slots, hidden), jnp.float32),
+            VMEM((slots, hidden), jnp.float32),
+            VMEM((slots, 256), jnp.float32),
+            VMEM((3, slots, hidden), bf16),
+            VMEM((parts, slots, width), bf16),
+            VMEM((max(parts // 2, 1), slots, width), bf16),
+            VMEM((extra, slots, width), bf16),
+            VMEM((extra, slots, width), bf16),
+            VMEM((slots, width), bf16),
+            VMEM((slots, width), bf16),
+            dma((2, experts)),
+            dma((2, experts)),
+            dma((2, hops, experts)),
+            dma((2, hops, experts)),
+            dma((2, max(parts // 2, 1))),
+            dma((extra, experts)),
+            dma((extra, experts)),
+            dma((experts,)),
+            dma((experts,)),
+            dma((experts // 2,)),
+            dma((experts // 2,)),
+            dma((3,)),
+            dma((5,)),
+            dma((2,)),
         ],
-        compiler_params=pltpu.CompilerParams(collective_id=1, has_side_effects=True),
-        name="combine",
-    )(partial, conv_out, mean, rstd, gain)
+        compiler_params=pltpu.CompilerParams(
+            collective_id=0, has_side_effects=True, vmem_limit_bytes=50 * 1024 * 1024
+        ),
+        name="front",
+    )(rows_send, cot_send, pick_t, cotangent, conv_out, mean, rstd, gain, gate, up, down)
+
+
+def grads_kernel(rows_ref, cot_ref, act_ref, gate_ref, up_ref, gate_out, up_out, down_out):
+    rows = rows_ref[...]
+    gate_out[...] = lax.dot_general(
+        rows, gate_ref[...], OUTER_DIMS, preferred_element_type=jnp.float32
+    ).astype(jnp.bfloat16)
+    up_out[...] = lax.dot_general(
+        rows, up_ref[...], OUTER_DIMS, preferred_element_type=jnp.float32
+    ).astype(jnp.bfloat16)
+    down_out[...] = lax.dot_general(
+        act_ref[...], cot_ref[...], OUTER_DIMS, preferred_element_type=jnp.float32
+    ).astype(jnp.bfloat16)
+
+
+def grads(rows, cot, act, gate_back, up_back):
+    parts, slots, width = rows.shape
+    hidden = act.shape[1]
+    piece = pl.BlockSpec((None, slots, width), lambda i: (i, 0, 0))
+    acts = pl.BlockSpec((slots, hidden), lambda i: (0, 0))
+    across = pl.BlockSpec((None, width, hidden), lambda i: (0, i, 0))
+    tall = jax.ShapeDtypeStruct((1, width * parts, hidden), jnp.bfloat16)
+    return pl.pallas_call(
+        grads_kernel,
+        grid=(parts,),
+        out_shape=(tall, tall, jax.ShapeDtypeStruct((1, hidden, width * parts), jnp.bfloat16)),
+        in_specs=[piece, piece, acts, acts, acts],
+        out_specs=[across, across, pl.BlockSpec((None, hidden, width), lambda i: (0, 0, i))],
+        name="grads",
+    )(rows, cot, act, gate_back, up_back)
 
 
 def tail_kernel(
@@ -546,11 +663,10 @@
     taps,
     out_proj,
 ):
-    tok_rows, local_width = out_cotangent.shape
+    tok_rows = out_cotangent.shape[0]
     experts = lax.axis_size("sp")
     parts = lax.axis_size("tp")
-    capacity = 3 * tok_rows // experts
-    full_width = local_width * parts
+    capacity = -(-3 * tok_rows // (experts * 16)) * 16
     slots = experts * capacity
 
     chosen = routes[:, :, None] == jnp.arange(experts, dtype=jnp.int32)[None, None, :]
@@ -569,49 +685,15 @@
         jnp.dot(pick, out_cotangent, preferred_element_type=jnp.float32)
         * slot_weight.reshape(slots, 1)
     ).astype(jnp.bfloat16)
-    arrived_rows, arrived_cot = dispatch(
-        send_rows.reshape(experts, capacity, local_width),
-        send_cot.reshape(experts, capacity, local_width),
-        experts, parts,
-    )
-    rows_in = arrived_rows.reshape(slots, full_width)
-    cot_in = arrived_cot.reshape(slots, full_width)
     mean, rstd, gain = conv_mean[None, :], conv_rstd[None, :], norm_gain[None, :]
-    gate_local = gate_proj[0]
-    up_local = up_proj[0]
-    down_local = down_proj[0]
-    gate_pre = jnp.dot(rows_in, gate_local, preferred_element_type=jnp.float32)
-    up_pre = jnp.dot(rows_in, up_local, preferred_element_type=jnp.float32)
-    gate_sigmoid = jax.nn.sigmoid(gate_pre)
-    activation = (gate_pre * gate_sigmoid * up_pre).astype(jnp.bfloat16)
-    act_grad = lax.dot_general(cot_in, down_local, INNER_DIMS, preferred_element_type=jnp.float32)
-    gate_back = (act_grad * up_pre * gate_sigmoid * (1.0 + gate_pre * (1.0 - gate_sigmoid))).astype(
-        jnp.bfloat16
-    )
-    up_back = (act_grad * gate_pre * gate_sigmoid).astype(jnp.bfloat16)
-    down_grad = lax.dot_general(
-        activation, cot_in, OUTER_DIMS, preferred_element_type=jnp.float32
-    ).astype(jnp.bfloat16)[None]
-    gate_grad = lax.dot_general(
-        rows_in, gate_back, OUTER_DIMS, preferred_element_type=jnp.float32
-    ).astype(jnp.bfloat16)[None]
-    up_grad = lax.dot_general(
-        rows_in, up_back, OUTER_DIMS, preferred_element_type=jnp.float32
-    ).astype(jnp.bfloat16)[None]
-    partial_rows = lax.dot_general(
-        gate_back, gate_local, INNER_DIMS, preferred_element_type=jnp.float32
-    )
-    partial_rows = partial_rows + lax.dot_general(
-        up_back, up_local, INNER_DIMS, preferred_element_type=jnp.float32
-    )
-    partial = partial_rows.astype(jnp.bfloat16).reshape(experts, capacity, full_width)
-    routed, near = combine(partial, conv_out, mean, rstd, gain, experts, parts)
-    routed = routed.reshape(slots, local_width)
-    routed_sum = lax.dot_general(pick, routed, OUTER_DIMS, preferred_element_type=jnp.float32)
-    stream = (out_cotangent.astype(jnp.float32) + routed_sum).astype(jnp.bfloat16)
+    rows, cot, act, gate_back, up_back, stream, stream_t, near = front(
+        send_rows, send_cot, pick.T, out_cotangent, conv_out, mean, rstd, gain,
+        gate_proj, up_proj, down_proj, experts, parts,
+    )
     conv_in_grad, proj_grad = tail(
-        stream.T, conv_out, mean, rstd, gain, taps, out_proj, near, experts, parts
-    )
+        stream_t, conv_out, mean, rstd, gain, taps, out_proj, near, experts, parts
+    )
+    gate_grad, up_grad, down_grad = grads(rows, cot, act, gate_back, up_back)
     return (gate_grad, up_grad, down_grad, proj_grad, stream, conv_in_grad)
 
 

time: 125 us -> 113 us (0.904)
  matrix products: 29.7 us -> 1.67 us
  Pallas kernels: 88 us -> 98.2 us
  local copies, waits for them, and re-layouts: 4.16 us -> 10.2 us
    dot_general x9 -> x0, matrix products: 26.7 us -> none  [the longest x1 4.44 us: body(): gate_pre = jnp.dot(rows_in, gate_local, preferred_element_type=jnp.float32)]
    pallas_call x2, Pallas kernels: 61.4 us -> 70.3 us  [the longest x1 60.7 us: front(): pl.pallas_call(functools.partial(front_kernel, experts, parts), out_shape...]
    unnamed x22 -> x29, local copies, waits for them, and re-layouts: 3.99 us -> 9.89 us
    pallas_call x1, Pallas kernels: 26.6 us -> 27.9 us  [tail(): pl.pallas_call(functools.partial(tail_kernel, experts, parts), out_shape=...]
where the time goes in v2:
time: 113 us; the launch traced here: 112 us
  Pallas kernels  98.2 us (87%)
  local copies, waits for them, and re-layouts  10.2 us (9%)
  matrix products  1.67 us (1%)
  other arithmetic  1.61 us (1%)
    pallas_call x1, Pallas kernels, front(): pl.pallas_call(functools.partial(front_kernel, experts, parts), out_shape...  60.7 us
    pallas_call x1, Pallas kernels, tail(): pl.pallas_call(functools.partial(tail_kernel, experts, parts), out_shape=...  27.9 us
    unnamed x29, local copies, waits for them, and re-layouts  9.89 us
    pallas_call x1, Pallas kernels, grads(): pl.pallas_call(grads_kernel, grid=(parts,), out_shape=(tall, tall, jax.Sh...  9.6 us

profile of v2, /device:TPU:0, one launch (start us, length us, event | category | flops | bytes accessed | tf_op | source)
XLA Modules:
  0.0 112.4 jit_solution(10821296480279844308)
XLA Ops:
  0.6 0.7 fusion.2
  1.4 0.1 fusion.1
  1.5 0.7 select_reduce_fusion.1
  2.2 0.1 select_reduce_fusion
  2.4 0.1 eq.44
  2.6 0.1 copy.25
  2.7 1.2 %fusion.cot_send_ref = bf16[384,512]{1,0:T(8,128)(2,1)S(1)} fusion(pred[384,128]{0,1:T(32,128)(4,1)S(1)} %get-tuple-element.33, bf16[128,512]{1,0:T(8,128)(2,1)} %cotangent_ref.1, f32[384]{0:T(512)S(1)} %mul.10), kind=kOutput, calls=%fused_computation.1 | convolution fusion | flops 50724864 | bytes 574976 | tf_op jit(solution)/shard_map/dot_general | solution.py:685
  4.0 0.3 convolution_convert_fusion.rows_send_ref
  4.3 0.9 copy-done.4
  5.2 0.9 copy-done.5
  6.1 0.7 copy-done.8
  6.8 0.7 copy-done.9
  7.4 0.7 copy-done.10
  8.1 60.7 %front.1 = (bf16[4,384,512]{2,1,0:T(8,128)(2,1)}, bf16[4,384,512]{2,1,0:T(8,128)(2,1)}, bf16[384,896]{1,0:T(8,128)(2,1)S(1)}, bf16[384,896]{1,0:T(8,128)(2,1)S(1...) custom-call(bf16[384,512]{1,0:T(8,128)(2,1)S(1)} %convolution_conver, ...), custom_call_target="tpu_custom_call" | custom-call | tf_op jit(solution)/shard_map/front/pallas_call | solution.py:387
  68.8 0.8 copy-done.1
  69.6 0.8 copy-done.2
  70.5 0.9 copy-done.3
  71.3 0.8 copy-done.6
  72.1 0.7 copy-done.7
  72.8 27.9 %tail.1 = (bf16[128,512]{1,0:T(8,128)(2,1)}, f32[256,512]{1,0:T(8,128)}) custom-call(bf16[512,128]{1,0:T(8,128)(2,1)} %copy-done.7, bf16[128,512]{1,0:T(8,128)(2,1)} %conv_out_ref.3, f32[1,128]{1,0:T(1,128)} %bitcast.16, f32[1,128]{1,0:T(1,128)} %bitcast.18, f32[1,512]{1,0:T(1,128)} %bitcast.14, f32[31,512]{1,0:T(8,128)} %taps_ref.1, ...), custom_call_target="tpu_custom_call" | custom-call | tf_op jit(solution)/shard_map/tail/pallas_call | solution.py:620
  100.7 9.6 %grads.1 = (bf16[1,2048,896]{2,1,0:T(8,128)(2,1)}, bf16[1,2048,896]{2,1,0:T(8,128)(2,1)}, bf16[1,896,2048]{2,1,0:T(8,128)(2,1)}) custom-call(bf16[4,384,512]{2,1,0:T(8,128)(2,1)} %get-tuple-element.19.rows_ref, bf16[4,384,512]{2,1,0:T(8,128)(2,1)} %get-tuple-element.20.cot_ref, bf16[384,896]{1,0:T(8,128)(2,1)} %copy-done.1, bf16[384,896]{1,0:T(8,128)(2,1)} %copy-done.2, ...), custom_call_target="tpu_custom_call" | custom-call | tf_op jit(solution)/shard_map/grads/pallas_call | solution.py:455
  110.3 0.8 copy.32
  111.1 0.7 copy.33
  111.8 0.7 copy.34
  (20 shorter events, 0.2 us)
Async XLA Ops:
  0.6 3.3 %copy-start = (bf16[128,512]{1,0:T(8,128)(2,1)S(1)}, bf16[128,512]{1,0:T(8,128)(2,1)}, u32[]{:S(2)}) copy-start(bf16[128,512]{1,0:T(8,128)(2,1)} %param.14) | copy-start | bytes 393220
  4.3 0.9 copy-start.4
  5.2 0.9 copy-start.5
  6.1 0.7 copy-start.8
  6.8 0.7 copy-start.9
  7.4 0.7 copy-start.10
  68.8 0.8 copy-start.1
  69.6 0.8 copy-start.2
  70.4 0.9 copy-start.3
  71.3 0.8 copy-start.6
  72.1 0.7 copy-start.7
  100.7 9.6 %copy-start.11 = (f32[256,512]{1,0:T(8,128)S(1)}, f32[256,512]{1,0:T(8,128)}, u32[]{:S(2)}) copy-start(f32[256,512]{1,0:T(8,128)} %get-tuple-element.43) | copy-start | bytes 1572868
  100.7 11.1 %copy-start.12 = (bf16[128,512]{1,0:T(8,128)(2,1)S(1)}, bf16[128,512]{1,0:T(8,128)(2,1)}, u32[]{:S(2)}) copy-start(bf16[128,512]{1,0:T(8,128)(2,1)} %get-tuple-element.45) | copy-start | bytes 393220

commit v3 on v2

--- a/solution.py
+++ b/solution.py
@@ -50,17 +50,12 @@
     return jnp.broadcast_to(row, (128, rows)).T[:, 0:1]
 
 
-def ladder(experts):
-    half = experts // 2
-    return list(range(half, experts)) + list(range(1, half))
-
-
 def front_kernel(
     experts, parts, rows_send_ref, cot_send_ref, pick_ref, cotangent_ref, conv_out_ref, mean_ref,
     rstd_ref, gain_ref, gate_hbm, up_hbm, down_hbm,
     rows_out, cot_out, act_out, gate_out, up_out, stream_ref, stream_t_ref, near_ref,
     gate, up, down, full, gate_pre, up_pre, act_grad, backs, partial, first_recv, recv, work, final,
-    routed, out_send, out_recv, hop_send, hop_recv, first_sems, back_send, back_recv, home_send,
+    routed, out_send, out_recv, hop_send, hop_recv, first_send, first_recv_sem, back_send, back_recv, home_send,
     home_recv, sw_send, sw_recv, weight_sem, save_sem, own_sem,
 ):
     me, col = lax.axis_index("sp"), lax.axis_index("tp")
@@ -93,6 +88,57 @@
             out_recv.at[kind, owner], (peer, col),
         )
 
+    held = [[col]]
+    for bit in bits:
+        held.append(held[-1] + [flipped(column, bit) for column in held[-1]])
+    starts, total = [], 0
+    for level in range(levels):
+        starts.append(total)
+        total += len(held[level])
+
+    def hop(kind, level, slot, column, source, own=False):
+        index = starts[level] + slot
+        src = place(kind, source, column)
+        if own:
+            src = sends[kind].at[block_rows(me), :]
+        return remote(
+            src, place(kind, source, column),
+            hop_send.at[kind, index, source], hop_recv.at[kind, index, source],
+            (me, flipped(col, bits[level])),
+        )
+
+    def hop_arrival(kind, level, slot, source):
+        return hop(kind, level, slot, flipped(held[level][slot], bits[level]), source)
+
+    def first_hops(kind, source, own=False):
+        for level in range(levels):
+            hop(kind, level, 0, col, source, own).start()
+
+    def arrive(kind, masks):
+        for mask in masks:
+            source = masked(me, mask)
+            out_copy(kind, source, source).wait_recv()
+            first_hops(kind, source)
+
+    def pass_on(kind, masks):
+        for level in range(1, levels):
+            size = len(held[level - 1])
+            for mask in masks:
+                source = masked(me, mask)
+                for slot in range(size):
+                    hop_arrival(kind, level - 1, slot, source).wait_recv()
+                for later in range(level, levels):
+                    for slot in range(size, 2 * size):
+                        hop(kind, later, slot, held[level][slot], source).start()
+
+    def collect(kind, masks):
+        for mask in masks:
+            source = masked(me, mask)
+            for slot in range(len(held[levels - 1])):
+                hop_arrival(kind, levels - 1, slot, source).wait_recv()
+
+    for kind in range(2):
+        first_hops(kind, me, True)
     for kind in range(2):
         for mask in range(1, experts):
             peer = masked(me, mask)
@@ -108,57 +154,6 @@
     for copy in own:
         copy.wait()
 
-    held = [[col]]
-    for bit in bits:
-        held.append(held[-1] + [flipped(column, bit) for column in held[-1]])
-    starts, total = [], 0
-    for level in range(levels):
-        starts.append(total)
-        total += len(held[level])
-
-    def hop(kind, level, slot, column, source):
-        index = starts[level] + slot
-        return remote(
-            place(kind, source, column), place(kind, source, column),
-            hop_send.at[kind, index, source], hop_recv.at[kind, index, source],
-            (me, flipped(col, bits[level])),
-        )
-
-    def hop_arrival(kind, level, slot, source):
-        return hop(kind, level, slot, flipped(held[level][slot], bits[level]), source)
-
-    def first_hops(kind, source):
-        for level in range(levels):
-            hop(kind, level, 0, col, source).start()
-
-    def arrive(kind):
-        for mask in range(1, experts):
-            source = masked(me, mask)
-            out_copy(kind, source, source).wait_recv()
-            first_hops(kind, source)
-
-    def pass_on(kind, masks, level):
-        size = len(held[level - 1])
-        for mask in masks:
-            source = masked(me, mask)
-            for slot in range(size):
-                hop_arrival(kind, level - 1, slot, source).wait_recv()
-            for later in range(level, levels):
-                for slot in range(size, 2 * size):
-                    hop(kind, later, slot, held[level][slot], source).start()
-
-    def collect(kind):
-        def step(k, carry):
-            source = lax.rem(me + k, experts)
-            for slot in range(len(held[levels - 1])):
-                hop_arrival(kind, levels - 1, slot, source).wait_recv()
-            return carry
-
-        lax.fori_loop(0, experts, step, 0)
-
-    for kind in range(2):
-        first_hops(kind, me)
-
     scaled = (
         (conv_out_ref[...].astype(jnp.float32) - column_of(mean_ref[...], tokens))
         * column_of(rstd_ref[...], tokens)
@@ -186,50 +181,38 @@
         for slot, source in enumerate(sources[level]):
             sw_copy(level, slot, flipped(source, far_bits[level])).wait_recv()
 
-    arrive(0)
-    arrive(1)
-    sw_start(0)
-    masks = list(range(experts))
-    for level in range(1, levels):
-        pass_on(0, masks, level)
-    collect(0)
-
-    def tiles(step):
-        whole = hidden // 256
-
-        def one(j, carry):
-            step(pl.ds(pl.multiple_of(j * 256, 256), 256), 256)
-            return carry
-
-        lax.fori_loop(0, whole, one, 0)
-        if hidden % 256:
-            step(pl.ds(whole * 256, hidden % 256), hidden % 256)
-
-    def joined(kind):
-        return jnp.concatenate([full[kind, part] for part in range(parts)], axis=1)
-
-    loads[0].wait()
-    loads[1].wait()
-
-    def pre(cols, size):
-        rows = joined(0)
+    def sw_pass():
+        sw_arrive(0)
+        if len(far_bits) > 1:
+            sw_start(1)
+
+    half = experts // 2
+    near, far = list(range(half)), list(range(half, experts))
+    own_half = me // half
+    span = half * capacity
+
+    def half_rows(side):
+        index = own_half if side == 0 else 1 - own_half
+        return pl.ds(pl.multiple_of(index * span, span), span)
+
+    def joined(kind, rows):
+        return jnp.concatenate([full[kind, part, rows, :] for part in range(parts)], axis=1)
+
+    def pre(cols):
+        rows = joined(0, slice(None))
         gate_pre[:, cols] = jnp.dot(rows, gate[:, cols], preferred_element_type=jnp.float32)
         up_pre[:, cols] = jnp.dot(rows, up[:, cols], preferred_element_type=jnp.float32)
 
-    tiles(pre)
-    for level in range(1, levels):
-        pass_on(1, masks, level)
-    collect(1)
-    loads[2].wait()
-
-    def back(cols, size):
+    def back_tile(side, cols, size):
         act_grad[:, 0:size] = lax.dot_general(
-            joined(1), down[cols, :], INNER_DIMS, preferred_element_type=jnp.float32
-        )
+            joined(1, half_rows(side)), down[cols, :], INNER_DIMS,
+            preferred_element_type=jnp.float32,
+        )
+        base = (own_half if side == 0 else 1 - own_half) * half
 
         def chunk(k, carry):
-            rows = block_rows(k)
-            gates, ups, grad = gate_pre[rows, cols], up_pre[rows, cols], act_grad[rows, 0:size]
+            rows = block_rows(base + k)
+            gates, ups, grad = gate_pre[rows, cols], up_pre[rows, cols], act_grad[block_rows(k), 0:size]
             sig = jax.nn.sigmoid(gates)
             silu = gates * sig
             backs[0, rows, cols] = (silu * ups).astype(jnp.bfloat16)
@@ -239,9 +222,102 @@
             backs[2, rows, cols] = (grad * silu).astype(jnp.bfloat16)
             return carry
 
-        lax.fori_loop(0, experts, chunk, 0)
-
-    tiles(back)
+        lax.fori_loop(0, half, chunk, 0)
+
+    def back(side):
+        def one(j, carry):
+            back_tile(side, pl.ds(pl.multiple_of(j * 256, 256), 256), 256)
+            return carry
+
+        lax.fori_loop(0, hidden // 256, one, 0)
+        if hidden % 256:
+            back_tile(side, pl.ds(hidden - hidden % 256, hidden % 256), hidden % 256)
+
+    arrive(0, range(1, experts))
+    arrive(1, near[1:])
+    pass_on(0, range(experts))
+    collect(0, range(experts))
+    loads[0].wait()
+    loads[1].wait()
+    tile_starts = list(range(0, hidden, 256))
+    waiting = list(far)
+    for index, start in enumerate(tile_starts):
+        upto = len(far) * (index + 1) // len(tile_starts)
+        arrive(1, far[len(far) - len(waiting) : upto])
+        waiting = far[upto:]
+        pre(pl.ds(start, min(256, hidden - start)))
+    sw_start(0)
+    pass_on(1, near)
+    collect(1, near)
+    loads[2].wait()
+    back(0)
+
+    kept = [[col]]
+    for bit in bits:
+        kept.insert(0, kept[0] + [flipped(column, bit) for column in kept[0]])
+    order = near[1:] + far + [0]
+
+    def first_copy(slot, side):
+        rows = half_rows(side)
+        return remote(
+            partial.at[flipped(kept[1][slot], up_bits[0]), rows, :], first_recv.at[slot, rows, :],
+            first_send.at[slot, side], first_recv_sem.at[slot, side],
+            (me, flipped(col, up_bits[0])),
+        )
+
+    def fill(column, side):
+        rows = pl.ds(pl.multiple_of(column * width, width), width)
+        tokens_at = slice(None) if side is None else half_rows(side)
+        value = lax.dot_general(
+            backs[1, tokens_at, :], gate[rows, :], INNER_DIMS, preferred_element_type=jnp.float32
+        ) + lax.dot_general(
+            backs[2, tokens_at, :], up[rows, :], INNER_DIMS, preferred_element_type=jnp.float32
+        )
+        partial[column, tokens_at, :] = value.astype(jnp.bfloat16)
+
+    back_starts, total = [0], 0
+    for level in range(1, levels):
+        back_starts.append(total)
+        total += len(kept[level + 1])
+
+    def back_copy(level, slot, block):
+        index = back_starts[level] + slot
+        return remote(
+            work.at[index, block_rows(block), :], recv.at[index, block_rows(block), :],
+            back_send.at[index, block], back_recv.at[index, block],
+            (me, flipped(col, up_bits[level])),
+        )
+
+    def summed(level, slot, block):
+        rows = block_rows(block)
+        value = partial[kept[level][slot], rows, :].astype(jnp.float32)
+        value = value + first_recv[slot, rows, :].astype(jnp.float32)
+        for stage in range(1, level):
+            value = value + recv[back_starts[stage] + slot, rows, :].astype(jnp.float32)
+        return value.astype(jnp.bfloat16)
+
+    size = len(kept[2]) if levels > 1 else 1
+    late_slots = list(range(size, len(kept[1])))
+
+    def fill_sent(side):
+        for slot in late_slots:
+            fill(flipped(kept[1][slot], up_bits[0]), side)
+            first_copy(slot, side).start()
+            fill(kept[1][slot], side)
+
+    def send_sums(side):
+        for slot in late_slots:
+            first_copy(slot, side).wait_recv()
+            for mask in (far if side else near):
+                block = masked(me, mask)
+                work[back_starts[1] + slot - size, block_rows(block), :] = summed(1, slot, block)
+                back_copy(1, slot - size, block).start()
+
+    fill_sent(0)
+    pass_on(1, far)
+    send_sums(0)
+    collect(1, far)
+    back(1)
     saves = [
         pltpu.make_async_copy(full.at[0], rows_out, save_sem.at[0]),
         pltpu.make_async_copy(full.at[1], cot_out, save_sem.at[1]),
@@ -249,61 +325,19 @@
         pltpu.make_async_copy(backs.at[1], gate_out, save_sem.at[3]),
         pltpu.make_async_copy(backs.at[2], up_out, save_sem.at[4]),
     ]
-
-    kept = [[col]]
-    for bit in bits:
-        kept.insert(0, kept[0] + [flipped(column, bit) for column in kept[0]])
-    order = ladder(experts) + [0]
-
-    def first_copy(slot):
-        return remote(
-            partial.at[flipped(kept[1][slot], up_bits[0])], first_recv.at[slot],
-            first_sems.at[0, slot], first_sems.at[1, slot], (me, flipped(col, up_bits[0])),
-        )
-
-    def fill(column):
-        rows = pl.ds(pl.multiple_of(column * width, width), width)
-        value = lax.dot_general(
-            backs[1], gate[rows, :], INNER_DIMS, preferred_element_type=jnp.float32
-        ) + lax.dot_general(
-            backs[2], up[rows, :], INNER_DIMS, preferred_element_type=jnp.float32
-        )
-        partial[column] = value.astype(jnp.bfloat16)
-
-    back_starts, total = [0], 0
-    for level in range(1, levels):
-        back_starts.append(total)
-        total += len(kept[level + 1])
-
-    def back_copy(level, slot, block):
-        index = back_starts[level] + slot
-        return remote(
-            work.at[index, block_rows(block), :], recv.at[index, block_rows(block), :],
-            back_send.at[index, block], back_recv.at[index, block],
-            (me, flipped(col, up_bits[level])),
-        )
-
-    def summed(level, slot, block):
-        rows = block_rows(block)
-        value = partial[kept[level][slot], rows, :].astype(jnp.float32)
-        value = value + first_recv[slot, rows, :].astype(jnp.float32)
-        for stage in range(1, level):
-            value = value + recv[back_starts[stage] + slot, rows, :].astype(jnp.float32)
-        return value.astype(jnp.bfloat16)
-
-    for slot in reversed(range(len(kept[1]))):
-        fill(flipped(kept[1][slot], up_bits[0]))
-        first_copy(slot).start()
-        fill(kept[1][slot])
-        first_copy(slot).wait_recv()
-        size = len(kept[2]) if levels > 1 else 0
-        if levels > 1 and slot >= size:
-            for mask in order:
-                block = masked(me, mask)
-                work[back_starts[1] + slot - size, block_rows(block), :] = summed(1, slot, block)
-                back_copy(1, slot - size, block).start()
+    fill_sent(1)
+    sw_pass()
+    send_sums(1)
     for copy in saves:
         copy.start()
+    for slot in reversed(range(size)):
+        fill(flipped(kept[1][slot], up_bits[0]), None)
+        for side in range(2):
+            first_copy(slot, side).start()
+        fill(kept[1][slot], None)
+    for slot in range(size):
+        for side in range(2):
+            first_copy(slot, side).wait_recv()
     for level in range(2, levels):
         size = len(kept[level + 1])
         for mask in order:
@@ -332,7 +366,7 @@
             home_copy(block, me).start()
         else:
             routed[block_rows(block), :] = value
-    for level in range(len(far_bits)):
+    for level in range(1, len(far_bits)):
         sw_arrive(level)
         if level + 1 < len(far_bits):
             sw_start(level + 1)
@@ -365,7 +399,8 @@
 
     lax.fori_loop(0, experts, finish, 0)
     for slot in range(len(kept[1])):
-        first_copy(slot).wait_send()
+        for side in range(2):
+            first_copy(slot, side).wait_send()
     for level in range(len(far_bits)):
         for slot, source in enumerate(sources[level]):
             sw_copy(level, slot, source).wait_send()
@@ -402,7 +437,7 @@
             VMEM((2, parts, slots, width), bf16),
             VMEM((slots, hidden), jnp.float32),
             VMEM((slots, hidden), jnp.float32),
-            VMEM((slots, 256), jnp.float32),
+            VMEM((slots // 2, 256), jnp.float32),
             VMEM((3, slots, hidden), bf16),
             VMEM((parts, slots, width), bf16),
             VMEM((max(parts // 2, 1), slots, width), bf16),
@@ -414,7 +449,8 @@
             dma((2, experts)),
             dma((2, hops, experts)),
             dma((2, hops, experts)),
-            dma((2, max(parts // 2, 1))),
+            dma((max(parts // 2, 1), 2)),
+            dma((max(parts // 2, 1), 2)),
             dma((extra, experts)),
             dma((extra, experts)),
             dma((experts,)),
@@ -426,7 +462,7 @@
             dma((2,)),
         ],
         compiler_params=pltpu.CompilerParams(
-            collective_id=0, has_side_effects=True, vmem_limit_bytes=50 * 1024 * 1024
+            collective_id=0, has_side_effects=True, vmem_limit_bytes=67_000_000
         ),
         name="front",
     )(rows_send, cot_send, pick_t, cotangent, conv_out, mean, rstd, gain, gate, up, down)
@@ -643,7 +679,9 @@
             pltpu.SemaphoreType.DMA((2,)),
             pltpu.SemaphoreType.DMA((2,)),
         ],
-        compiler_params=pltpu.CompilerParams(collective_id=2, has_side_effects=True),
+        compiler_params=pltpu.CompilerParams(
+            collective_id=2, has_side_effects=True, vmem_limit_bytes=67_000_000
+        ),
         name="tail",
     )(stream_t, conv_out, mean, rstd, gain, taps, proj, near)
 

time: 113 us -> 106 us (0.938)
  local copies, waits for them, and re-layouts: 10.2 us -> 2.42 us
  matrix products: 1.67 us -> 4.07 us
  Pallas kernels: 98.2 us -> 96.6 us
    unnamed x29 -> x9, local copies, waits for them, and re-layouts: 9.89 us -> 2.12 us
    dot_general x1, matrix products: 0.31 us -> 1.97 us  [body(): jnp.dot(pick, expert_input, preferred_element_type=jnp.float32)]
    pallas_call x1, Pallas kernels: 60.7 us -> 59 us  [front(): pl.pallas_call(functools.partial(front_kernel, experts, parts), out_shape...]
where the time goes in v3:
time: 106 us
  Pallas kernels  96.6 us (91%)
  matrix products  4.07 us (4%)
  local copies, waits for them, and re-layouts  2.42 us (2%)
  other arithmetic  2.22 us (2%)
    pallas_call x1, Pallas kernels, front(): pl.pallas_call(functools.partial(front_kernel, experts, parts), out_shape...  59 us
    pallas_call x1, Pallas kernels, tail(): pl.pallas_call(functools.partial(tail_kernel, experts, parts), out_shape=...  28 us
    pallas_call x1, Pallas kernels, grads(): pl.pallas_call(grads_kernel, grid=(parts,), out_shape=(tall, tall, jax.Sh...  9.61 us

profile of v3, /device:TPU:0, one launch (start us, length us, event | category | flops | bytes accessed | tf_op | source)
XLA Modules:
  0.0 106.0 jit_solution(7765344975271544873)
XLA Ops:
  0.6 0.7 fusion.2
  1.3 0.1 fusion.1
  1.5 0.7 select_reduce_fusion.1
  2.2 0.1 select_reduce_fusion
  2.3 0.1 mul.10
  2.4 0.1 eq.44
  2.5 0.1 copy.25
  2.6 0.7 convert_bitcast_fusion
  3.3 2.0 %fusion.cot_send_ref = bf16[384,512]{1,0:T(8,128)(2,1)} fusion(pred[384,128]{0,1:T(32,128)(4,1)S(1)} %get-tuple-element.33, bf16[128,512]{1,0:T(8,128)(2,1)} %cotangent_ref.1, f32[384]{0:T(512)S(1)} %mul.10), kind=kOutput, calls=%fused_computation.1 | convolution fusion | flops 50724864 | bytes 574976 | tf_op jit(solution)/shard_map/dot_general | solution.py:723
  5.3 2.0 %convolution_convert_fusion.rows_send_ref = bf16[384,512]{1,0:T(8,128)(2,1)} fusion(pred[384,128]{0,1:T(32,128)(4,1)S(1)} %get-tuple-element.33, bf16[128,512]{1,0:T(8,128)(2,1)} %param.14), kind=kOutput, calls=%fused_computation.2 | convolution fusion | flops 50528256 | bytes 573440 | tf_op jit(solution)/shard_map/dot_general | solution.py:721
  7.3 59.0 %front.1 = (bf16[4,384,512]{2,1,0:T(8,128)(2,1)}, bf16[4,384,512]{2,1,0:T(8,128)(2,1)}, bf16[384,896]{1,0:T(8,128)(2,1)}, bf16[384,896]{1,0:T(8,128)(2,1)}, bf16...) custom-call(bf16[384,512]{1,0:T(8,128)(2,1)} %convolution_convert_fusi, ...), custom_call_target="tpu_custom_call" | custom-call | tf_op jit(solution)/shard_map/front/pallas_call | solution.py:422
  66.3 28.0 %tail.1 = (bf16[128,512]{1,0:T(8,128)(2,1)}, f32[256,512]{1,0:T(8,128)}) custom-call(bf16[512,128]{1,0:T(8,128)(2,1)} %get-tuple-element.27.stream_ref, bf16[128,512]{1,0:T(8,128)(2,1)} %conv_out_ref.3, f32[1,128]{1,0:T(1,128)} %bitcast.19, f32[1,128]{1,0:T(1,128)} %bitcast.21, f32[1,512]{1,0:T(1,128)} %bitcast.17, f32[31,512]{1,0:T(8,128)} %taps_ref.1, ...), custom_call_target="tpu_custom_call" | custom-call | tf_op jit(solution)/shard_map/tail/pallas_call | solution.py:656
  94.3 0.0 copy-start
  94.3 0.0 copy-start.1
  94.3 0.0 copy-start.2
  94.3 9.6 %grads.1 = (bf16[1,2048,896]{2,1,0:T(8,128)(2,1)}, bf16[1,2048,896]{2,1,0:T(8,128)(2,1)}, bf16[1,896,2048]{2,1,0:T(8,128)(2,1)}) custom-call(bf16[4,384,512]{2,1,0:T(8,128)(2,1)} %get-tuple-element.19.rows_ref, bf16[4,384,512]{2,1,0:T(8,128)(2,1)} %get-tuple-element.20.cot_ref, bf16[384,896]{1,0:T(8,128)(2,1)} %get-tuple-element.21.act_ref, ...), custom_call_target="tpu_custom_call" | custom-call | tf_op jit(solution)/shard_map/grads/pallas_call | solution.py:491
  103.9 0.0 copy-done
  103.9 0.8 copy.32
  104.7 0.0 copy-done.1
  104.7 0.7 copy.33
  105.4 0.0 copy-done.2
  105.4 0.7 copy.34
  (2 shorter events, 0.0 us)
Async XLA Ops:
  94.3 9.6 %copy-start = (f32[256,512]{1,0:T(8,128)S(1)}, f32[256,512]{1,0:T(8,128)}, u32[]{:S(2)}) copy-start(f32[256,512]{1,0:T(8,128)} %get-tuple-element.43) | copy-start | bytes 1572868
  94.3 10.4 %copy-start.1 = (bf16[128,512]{1,0:T(8,128)(2,1)S(1)}, bf16[128,512]{1,0:T(8,128)(2,1)}, u32[]{:S(2)}) copy-start(bf16[128,512]{1,0:T(8,128)(2,1)} %get-tuple-element.44) | copy-start | bytes 393220
  94.3 11.1 %copy-start.2 = (bf16[128,512]{1,0:T(8,128)(2,1)S(1)}, bf16[128,512]{1,0:T(8,128)(2,1)}, u32[]{:S(2)}) copy-start(bf16[128,512]{1,0:T(8,128)(2,1)} %get-tuple-element.45) | copy-start | bytes 393220

commit v4 on v3

--- a/solution.py
+++ b/solution.py
@@ -32,11 +32,14 @@
     return bits
 
 
-def greet(devices):
+def hail(devices):
     barrier = pltpu.get_barrier_semaphore()
     for device in devices:
         pl.semaphore_signal(barrier, inc=1, device_id=device, device_id_type=MESH)
-    pl.semaphore_wait(barrier, len(devices))
+
+
+def gather_hails(count):
+    pl.semaphore_wait(pltpu.get_barrier_semaphore(), count)
 
 
 def remote(src, dst, send_sem, recv_sem, device):
@@ -50,47 +53,87 @@
     return jnp.broadcast_to(row, (128, rows)).T[:, 0:1]
 
 
-def front_kernel(
-    experts, parts, rows_send_ref, cot_send_ref, pick_ref, cotangent_ref, conv_out_ref, mean_ref,
-    rstd_ref, gain_ref, gate_hbm, up_hbm, down_hbm,
-    rows_out, cot_out, act_out, gate_out, up_out, stream_ref, stream_t_ref, near_ref,
-    gate, up, down, full, gate_pre, up_pre, act_grad, backs, partial, first_recv, recv, work, final,
-    routed, out_send, out_recv, hop_send, hop_recv, first_send, first_recv_sem, back_send, back_recv, home_send,
-    home_recv, sw_send, sw_recv, weight_sem, save_sem, own_sem,
+def step_kernel(
+    experts, parts, tokens_ref, cotangent_ref, routes_ref, weights_ref, conv_out_ref, mean_ref,
+    rstd_ref, gain_ref, taps_ref, gate_hbm, up_hbm, down_hbm, proj_hbm,
+    rows_out, cot_out, act_out, gate_out, up_out, stream_ref, conv_ref, proj_grad_ref,
+    pick, rows_send_ref, cot_send_ref, gate, up, down, proj, full, gate_pre, up_pre, act_grad, backs,
+    partial, first_recv, recv, work, final, routed, swish, stream_t, whole, arrived, grads, scaled_norm,
+    extended, halo_grads, halo_norms, stats, next_stats,
+    out_send, out_recv, hop_send, hop_recv, first_send, first_recv_sem, back_send,
+    back_recv, home_send, home_recv, sw_send, sw_recv, side_send, side_recv, ring_send, ring_recv,
+    piece_send, piece_recv, twin_send, twin_recv, stat_send, stat_recv, next_send, next_recv,
+    halo_sem, weight_sem, save_sem, own_sem,
 ):
     me, col = lax.axis_index("sp"), lax.axis_index("tp")
-    width = rows_send_ref.shape[1]
-    capacity = rows_send_ref.shape[0] // experts
+    tokens, width = tokens_ref.shape
+    capacity = pick.shape[0] // experts
     hidden = gate.shape[1]
-    tokens = conv_out_ref.shape[0]
+    piece = width * parts // experts
+    per_column = width // piece
+    halo = halo_grads.shape[0]
     up_bits = bits_of(parts)
     bits = up_bits[::-1]
     levels = len(bits)
     loads = []
-    for index, (src, dst) in enumerate(((gate_hbm, gate), (up_hbm, up), (down_hbm, down))):
-        loads.append(pltpu.make_async_copy(src.at[0], dst, weight_sem.at[index]))
+    for index, (src, dst) in enumerate(
+        ((gate_hbm.at[0], gate), (up_hbm.at[0], up), (down_hbm.at[0], down), (proj_hbm, proj))
+    ):
+        loads.append(pltpu.make_async_copy(src, dst, weight_sem.at[index]))
         loads[-1].start()
-    greet(
-        [(lax.rem(me + k, experts), col) for k in range(1, experts)]
-        + [(me, flipped(col, bit)) for bit in bits]
-    )
-    sends = (rows_send_ref, cot_send_ref)
-
-    def block_rows(source):
-        return pl.ds(pl.multiple_of(source * capacity, capacity), capacity)
-
-    def place(kind, source, column):
-        return full.at[kind, column, block_rows(source), :]
-
-    def out_copy(kind, peer, owner):
-        return remote(
-            sends[kind].at[block_rows(peer), :], place(kind, owner, col), out_send.at[kind, peer],
-            out_recv.at[kind, owner], (peer, col),
-        )
-
     held = [[col]]
     for bit in bits:
         held.append(held[-1] + [flipped(column, bit) for column in held[-1]])
+    twins = held[levels - 1]
+    others = [flipped(column, bits[-1]) for column in twins]
+    peers = [(lax.rem(me + k, experts), column) for k in range(1, experts) for column in twins]
+    peers += [(me, column) for column in twins[1:] + others]
+    peers += [(lax.rem(me + k, experts), column) for k in (1, experts - 1) for column in others]
+    hail(peers)
+
+    expert_at = lax.broadcasted_iota(jnp.int32, (experts, tokens), 0)
+    first, second = routes_ref[0:1, :] == expert_at, routes_ref[1:2, :] == expert_at
+    weight = jnp.where(first, weights_ref[0:1, :], 0.0) + jnp.where(second, weights_ref[1:2, :], 0.0)
+    named = jnp.where(first | second, 1.0, 0.0)
+    before = jnp.where(
+        lax.broadcasted_iota(jnp.int32, (tokens, tokens), 0)
+        < lax.broadcasted_iota(jnp.int32, (tokens, tokens), 1),
+        1.0, 0.0,
+    ).astype(jnp.bfloat16)
+    rank = jnp.dot(named.astype(jnp.bfloat16), before, preferred_element_type=jnp.float32)
+    rank = jnp.where(first | second, rank.astype(jnp.int32), -1)
+    slot_at = lax.broadcasted_iota(jnp.int32, (capacity, tokens), 0)
+    slot_weights = []
+    for expert in range(experts):
+        chosen = rank[expert : expert + 1, :] == slot_at
+        pick[pl.ds(expert * capacity, capacity), :] = jnp.where(chosen, 1.0, 0.0).astype(jnp.bfloat16)
+        slot_weights.append(
+            jnp.sum(jnp.where(chosen, weight[expert : expert + 1, :], 0.0), axis=1, keepdims=True)
+        )
+    rows_send_ref[...] = jnp.dot(
+        pick[...], tokens_ref[...], preferred_element_type=jnp.float32
+    ).astype(jnp.bfloat16)
+    for expert in range(experts):
+        mine = pl.ds(expert * capacity, capacity)
+        cot_send_ref[mine, :] = (
+            jnp.dot(pick[mine, :], cotangent_ref[...], preferred_element_type=jnp.float32)
+            * slot_weights[expert]
+        ).astype(jnp.bfloat16)
+    gather_hails(len(peers))
+    sends = (rows_send_ref, cot_send_ref)
+
+    def block_rows(source):
+        return pl.ds(pl.multiple_of(source * capacity, capacity), capacity)
+
+    def place(kind, source, column):
+        return full.at[kind, column, block_rows(source), :]
+
+    def out_copy(kind, peer, owner):
+        return remote(
+            sends[kind].at[block_rows(peer), :], place(kind, owner, col), out_send.at[kind, peer],
+            out_recv.at[kind, owner], (peer, col),
+        )
+
     starts, total = [], 0
     for level in range(levels):
         starts.append(total)
@@ -154,12 +197,32 @@
     for copy in own:
         copy.wait()
 
-    scaled = (
-        (conv_out_ref[...].astype(jnp.float32) - column_of(mean_ref[...], tokens))
-        * column_of(rstd_ref[...], tokens)
-        * gain_ref[...]
-    )
-    near_ref[me // 2] = (scaled * jax.nn.sigmoid(scaled)).astype(jnp.bfloat16)
+    gain = gain_ref[...]
+    rstd = column_of(rstd_ref[...], tokens)
+    normed = (conv_out_ref[...].astype(jnp.float32) - column_of(mean_ref[...], tokens)) * rstd
+    scaled = normed * gain
+    swish[me] = (scaled * jax.nn.sigmoid(scaled)).astype(jnp.bfloat16)
+    scaled_norm[...] = rstd * normed
+
+    before_me = lax.rem(me + experts - 1, experts)
+
+    def halo_copy(index, src, dst):
+        return remote(
+            src.at[pl.ds(0, halo), :], dst, halo_sem.at[index, 0], halo_sem.at[index, 1],
+            (before_me, col),
+        )
+
+    @pl.when(me > 0)
+    def _():
+        halo_copy(0, scaled_norm, halo_norms).start()
+
+    def side_copy(source):
+        return remote(
+            swish.at[source], swish.at[source], side_send.at[source], side_recv.at[source],
+            (flipped(me, 1), col),
+        )
+
+    side_copy(me).start()
 
     far_bits = bits_of(experts)[:0:-1]
     sources = [[me]]
@@ -169,7 +232,7 @@
     def sw_copy(level, slot, source):
         index = (1 << level) - 1 + slot
         return remote(
-            near_ref.at[source // 2], near_ref.at[source // 2], sw_send.at[index],
+            swish.at[source], swish.at[source], sw_send.at[index],
             sw_recv.at[index], (flipped(me, far_bits[level]), col),
         )
 
@@ -180,6 +243,7 @@
     def sw_arrive(level):
         for slot, source in enumerate(sources[level]):
             sw_copy(level, slot, flipped(source, far_bits[level])).wait_recv()
+            side_copy(flipped(source, far_bits[level])).start()
 
     def sw_pass():
         sw_arrive(0)
@@ -373,11 +437,218 @@
     for mask in order[:-1]:
         source = masked(me, mask)
         home_copy(source, source).wait_recv()
-    stream = cotangent_ref[...].astype(jnp.float32) + jnp.dot(
-        pick_ref[...], routed[...], preferred_element_type=jnp.float32
+    stream = cotangent_ref[...].astype(jnp.float32) + lax.dot_general(
+        pick[...], routed[...], OUTER_DIMS, preferred_element_type=jnp.float32
     )
+    whole[col] = stream.astype(jnp.bfloat16)
+    stream_t[...] = stream.T.astype(jnp.bfloat16)
+
+    def ring(level, slot, column):
+        index = starts[level] + slot
+        return remote(
+            whole.at[column], whole.at[column], ring_send.at[index], ring_recv.at[index],
+            (me, flipped(col, bits[level])),
+        )
+
+    def ring_arrival(level, slot):
+        return ring(level, slot, flipped(held[level][slot], bits[level]))
+
+    for level in range(levels):
+        ring(level, 0, col).start()
+
+    def landing(source):
+        return arrived.at[:, pl.ds(pl.multiple_of(source * tokens, tokens), tokens)]
+
+    def piece_copy(j, slot, source, owner):
+        index = j * len(twins) + slot
+        return remote(
+            stream_t.at[pl.ds(j * piece, piece), :], landing(owner), piece_send.at[index],
+            piece_recv.at[source], (col * per_column + j, twins[slot]),
+        )
+
+    def own_piece(j):
+        return pltpu.make_async_copy(
+            stream_t.at[pl.ds(j * piece, piece), :], landing(me), own_sem.at[0]
+        )
+
+    for slot in reversed(range(len(twins))):
+        for j in range(per_column):
+            if slot:
+                piece_copy(j, slot, me, me).start()
+            else:
+
+                @pl.when(col * per_column + j != me)
+                def _(j=j):
+                    piece_copy(j, 0, me, me).start()
+
+                @pl.when(col * per_column + j == me)
+                def _(j=j):
+                    own_piece(j).start()
+                    own_piece(j).wait()
+
     stream_ref[...] = stream.astype(jnp.bfloat16)
-    stream_t_ref[...] = stream.T.astype(jnp.bfloat16)
+    loads[3].wait()
+
+    def through(column):
+        rows = pl.ds(pl.multiple_of(column * width, width), width)
+        return jnp.dot(whole[column], proj[rows, :], preferred_element_type=jnp.float32)
+
+    grads[...] = through(col)
+    for level in range(1, levels):
+        size = len(held[level - 1])
+        for slot in range(size):
+            ring_arrival(level - 1, slot).wait_recv()
+        for later in range(level, levels):
+            for slot in range(size, 2 * size):
+                ring(later, slot, held[level][slot]).start()
+        for slot in range(size):
+            grads[...] += through(flipped(held[level - 1][slot], bits[level - 1]))
+    for slot in range(len(held[levels - 1])):
+        ring_arrival(levels - 1, slot).wait_recv()
+        grads[...] += through(flipped(held[levels - 1][slot], bits[levels - 1]))
+    gain = gain_ref[...]
+    rstd = column_of(rstd_ref[...], tokens)
+    normed = (conv_out_ref[...].astype(jnp.float32) - column_of(mean_ref[...], tokens)) * rstd
+    scaled = normed * gain
+    sig = jax.nn.sigmoid(scaled)
+    scaled_grad = grads[...] * sig * (1.0 + scaled * (1.0 - sig)) * gain
+    grads[...] = rstd * scaled_grad
+
+    @pl.when(me > 0)
+    def _():
+        halo_copy(1, grads, halo_grads).start()
+
+    first_sum = jnp.sum(scaled_grad, axis=1, keepdims=True)
+    second_sum = jnp.sum(scaled_grad * normed, axis=1, keepdims=True)
+    lane = lax.broadcasted_iota(jnp.int32, (tokens, 128), 1)
+    table = jnp.where(lane == 0, first_sum, jnp.where(lane == 1, second_sum, rstd))
+    stats[0] = table.T[:8]
+
+    def stat_copy(k):
+        return remote(
+            stats.at[0], stats.at[k], stat_send.at[k], stat_recv.at[k],
+            (me, lax.rem(col + k, parts)),
+        )
+
+    def next_copy(k):
+        return remote(
+            stats.at[0], next_stats.at[k], next_send.at[k], next_recv.at[k],
+            (before_me, lax.rem(col + k, parts)),
+        )
+
+    for k in range(1, parts):
+        stat_copy(k).start()
+
+    @pl.when(me > 0)
+    def _():
+        for k in range(parts):
+            next_copy(k).start()
+
+    direct = lax.rem(me // per_column, 2) == lax.rem(col, 2)
+    twin = flipped(col, 1)
+
+    def twin_copy(source):
+        return remote(
+            landing(source), landing(source), twin_send.at[source], twin_recv.at[source], (me, twin)
+        )
+
+    @pl.when(direct)
+    def _():
+        for mask in range(experts):
+            source = masked(me, mask)
+            if mask:
+                piece_copy(0, 0, source, source).wait_recv()
+            else:
+
+                @pl.when(me // per_column != col)
+                def _():
+                    piece_copy(0, 0, me, me).wait_recv()
+
+            twin_copy(source).start()
+
+    def means(refs):
+        total = refs[0]
+        for k in range(1, parts):
+            total = total + refs[k]
+        return jnp.concatenate([total / (width * parts)] * 16, axis=0).T
+
+    for k in range(1, parts):
+        stat_copy(k).wait_recv()
+    spread = means(stats)
+    extended[0:tokens, :] = (
+        grads[...] - rstd * spread[:, 0:1] - scaled_norm[...] * spread[:, 1:2]
+    )
+
+    def conv(start, size):
+        for lanes in range(0, width, 128):
+            cols = pl.ds(lanes, 128)
+            total = jnp.zeros((size, 128), jnp.float32)
+            for offset in range(taps_ref.shape[0]):
+                total = total + (
+                    taps_ref[offset : offset + 1, cols] * extended[pl.ds(start + offset, size), cols]
+                )
+            conv_ref[pl.ds(start, size), cols] = total.astype(jnp.bfloat16)
+
+    conv(0, tokens - halo)
+
+    @pl.when(me == experts - 1)
+    def _():
+        extended[tokens:, :] = jnp.zeros((halo, width), jnp.float32)
+
+    @pl.when(me < experts - 1)
+    def _():
+        halo_copy(0, scaled_norm, halo_norms).wait_recv()
+        halo_copy(1, grads, halo_grads).wait_recv()
+        for k in range(parts):
+            next_copy(k).wait_recv()
+        after = means(next_stats)[0:halo]
+        extended[tokens:, :] = (
+            halo_grads[...] - (after[:, 2:3] * width) * after[:, 0:1] - halo_norms[...] * after[:, 1:2]
+        )
+
+    conv(tokens - halo, halo)
+    for source in sources[-1]:
+        side_copy(flipped(source, 1)).wait_recv()
+
+    @pl.when(jnp.logical_not(direct))
+    def _():
+        for mask in range(experts):
+            twin_copy(masked(me, mask)).wait_recv()
+
+    proj_grad_ref[...] = jnp.dot(
+        arrived[...], swish[...].reshape(experts * tokens, width), preferred_element_type=jnp.float32
+    )
+
+    @pl.when(direct)
+    def _():
+        for mask in range(experts):
+            twin_copy(masked(me, mask)).wait_send()
+
+    for k in range(1, parts):
+        stat_copy(k).wait_send()
+
+    @pl.when(me > 0)
+    def _():
+        halo_copy(0, scaled_norm, halo_norms).wait_send()
+        halo_copy(1, grads, halo_grads).wait_send()
+        for k in range(parts):
+            next_copy(k).wait_send()
+
+    for level in range(levels):
+        for slot in range(len(held[level])):
+            ring(level, slot, held[level][slot]).wait_send()
+    for slot in range(len(twins)):
+        for j in range(per_column):
+            if slot:
+                piece_copy(j, slot, me, me).wait_send()
+            else:
+
+                @pl.when(col * per_column + j != me)
+                def _(j=j):
+                    piece_copy(j, 0, me, me).wait_send()
+
+    for source in sources[-1]:
+        side_copy(source).wait_send()
 
     def finish(k, carry):
         source = lax.rem(me + k, experts)
@@ -408,64 +679,99 @@
         copy.wait()
 
 
-def front(
-    rows_send, cot_send, pick_t, cotangent, conv_out, mean, rstd, gain, gate, up, down, experts, parts
+def step(
+    tokens_in, cotangent, routes_t, weights_t, conv_out, mean, rstd, gain, taps, gate, up, down, proj,
+    experts, parts,
 ):
-    slots, width = rows_send.shape
+    tokens, width = cotangent.shape
+    slots = experts * (-(-3 * tokens // (experts * 16)) * 16)
     full_width, hidden = gate.shape[1:]
-    tokens = conv_out.shape[0]
+    block = full_width // experts
+    halo = -(-(taps.shape[0] - 1) // 8) * 8
     hops = parts - 1
-    extra = max(parts // 2 - 1, 1)
-    bf16, dma = jnp.bfloat16, pltpu.SemaphoreType.DMA
+    half = max(parts // 2, 1)
+    extra = max(half - 1, 1)
+    bf16, f32, dma = jnp.bfloat16, jnp.float32, pltpu.SemaphoreType.DMA
     rows_all = jax.ShapeDtypeStruct((parts, slots, width), bf16)
     acts = jax.ShapeDtypeStruct((slots, hidden), bf16)
+    in_vmem, anywhere = pl.BlockSpec(memory_space=VMEM), pl.BlockSpec(memory_space=pl.ANY)
     return pl.pallas_call(
-        functools.partial(front_kernel, experts, parts),
+        functools.partial(step_kernel, experts, parts),
         out_shape=(
             rows_all, rows_all, acts, acts, acts,
             jax.ShapeDtypeStruct((tokens, width), bf16),
-            jax.ShapeDtypeStruct((width, tokens), bf16),
-            jax.ShapeDtypeStruct((experts // 2, tokens, width), bf16),
+            jax.ShapeDtypeStruct((tokens, width), bf16),
+            jax.ShapeDtypeStruct((block, width), f32),
         ),
-        in_specs=[pl.BlockSpec(memory_space=VMEM)] * 8 + [pl.BlockSpec(memory_space=pl.ANY)] * 3,
-        out_specs=[pl.BlockSpec(memory_space=pl.ANY)] * 5
-        + [pl.BlockSpec(memory_space=VMEM)] * 3,
+        in_specs=[in_vmem] * 9 + [anywhere] * 4,
+        out_specs=[anywhere] * 5 + [in_vmem] * 3,
         scratch_shapes=[
+            VMEM((slots, tokens), bf16),
+            VMEM((slots, width), bf16),
+            VMEM((slots, width), bf16),
             VMEM((full_width, hidden), bf16),
             VMEM((full_width, hidden), bf16),
             VMEM((hidden, full_width), bf16),
+            VMEM((full_width, width), bf16),
             VMEM((2, parts, slots, width), bf16),
-            VMEM((slots, hidden), jnp.float32),
-            VMEM((slots, hidden), jnp.float32),
-            VMEM((slots // 2, 256), jnp.float32),
+            VMEM((slots, hidden), f32),
+            VMEM((slots, hidden), f32),
+            VMEM((slots // 2, 256), f32),
             VMEM((3, slots, hidden), bf16),
             VMEM((parts, slots, width), bf16),
-            VMEM((max(parts // 2, 1), slots, width), bf16),
+            VMEM((half, slots, width), bf16),
             VMEM((extra, slots, width), bf16),
             VMEM((extra, slots, width), bf16),
             VMEM((slots, width), bf16),
             VMEM((slots, width), bf16),
+            VMEM((experts, tokens, width), bf16),
+            VMEM((width, tokens), bf16),
+            VMEM((parts, tokens, width), bf16),
+            VMEM((block, experts * tokens), bf16),
+            VMEM((tokens, width), f32),
+            VMEM((tokens, width), f32),
+            VMEM((tokens + halo, width), f32),
+            VMEM((halo, width), f32),
+            VMEM((halo, width), f32),
+            VMEM((parts, 8, tokens), f32),
+            VMEM((parts, 8, tokens), f32),
             dma((2, experts)),
             dma((2, experts)),
             dma((2, hops, experts)),
             dma((2, hops, experts)),
-            dma((max(parts // 2, 1), 2)),
-            dma((max(parts // 2, 1), 2)),
+            dma((half, 2)),
+            dma((half, 2)),
             dma((extra, experts)),
             dma((extra, experts)),
             dma((experts,)),
             dma((experts,)),
             dma((experts // 2,)),
             dma((experts // 2,)),
-            dma((3,)),
+            dma((experts,)),
+            dma((experts,)),
+            dma((hops,)),
+            dma((hops,)),
+            dma((width // block * half,)),
+            dma((experts,)),
+            dma((experts,)),
+            dma((experts,)),
+            dma((parts,)),
+            dma((parts,)),
+            dma((parts,)),
+            dma((parts,)),
+            dma((2, 2)),
+            dma((4,)),
             dma((5,)),
             dma((2,)),
         ],
         compiler_params=pltpu.CompilerParams(
             collective_id=0, has_side_effects=True, vmem_limit_bytes=67_000_000
         ),
-        name="front",
-    )(rows_send, cot_send, pick_t, cotangent, conv_out, mean, rstd, gain, gate, up, down)
+        name="step",
+    )(
+        tokens_in, cotangent, routes_t, weights_t, conv_out, mean, rstd, gain, taps,
+        gate, up, down, proj,
+    )
 
 
 def grads_kernel(rows_ref, cot_ref, act_ref, gate_ref, up_ref, gate_out, up_out, down_out):
@@ -498,194 +804,6 @@
     )(rows, cot, act, gate_back, up_back)
 
 
-def tail_kernel(
-    experts, parts, stream_ref, conv_out_ref, mean_ref, rstd_ref, gain_ref, taps_ref, proj_ref,
-    near_ref, conv_ref, proj_grad_ref,
-    whole, arrived, far, extended, stats, grads, norms,
-    hop_send, hop_recv, out_send, out_recv, stat_send, stat_recv, halo_sem, local_sem, far_sem,
-):
-    me, col = lax.axis_index("sp"), lax.axis_index("tp")
-    width, rows = stream_ref.shape
-    full = width * parts
-    block = full // experts
-    bits = bits_of(parts)[::-1]
-    tap_count = taps_ref.shape[0]
-    halo = extended.shape[0] - rows
-    greet(
-        [(lax.rem(me + k, experts), col) for k in range(1, experts)]
-        + [(me, lax.rem(col + k, parts)) for k in range(1, parts)]
-    )
-
-    far_copy = remote(near_ref, far, far_sem.at[0], far_sem.at[1], (flipped(me, 1), col))
-    far_copy.start()
-
-    def part(column):
-        return whole.at[pl.ds(pl.multiple_of(column * width, width), width), :]
-
-    own = pltpu.make_async_copy(stream_ref, part(col), local_sem.at[0])
-    own.start()
-    index, held, copies = 0, [col], []
-    for level, bit in enumerate(bits):
-        for slot, column in enumerate(held):
-            src = stream_ref if column is col else part(column)
-            copy = remote(
-                src, part(column), hop_send.at[index + slot], hop_recv.at[index + slot],
-                (me, flipped(col, bit)),
-            )
-            copy.start()
-            copies.append(copy)
-        for slot in range(len(held)):
-            column = flipped(held[slot], bit)
-            remote(
-                part(column), part(column), hop_send.at[index + slot], hop_recv.at[index + slot],
-                (me, flipped(col, bit)),
-            ).wait_recv()
-        index += len(held)
-        held = held + [flipped(column, bit) for column in held]
-    own.wait()
-
-    def piece(peer):
-        return whole.at[pl.ds(pl.multiple_of(peer * block, block), block), :]
-
-    def landing(receiver, source):
-        slot = lax.rem(receiver + source, 2) * (experts // 2) + source // 2
-        return arrived.at[:, pl.ds(pl.multiple_of(slot * rows, rows), rows)]
-
-    def out_copy(peer):
-        return remote(piece(peer), landing(peer, me), out_send.at[peer], out_recv.at[me], (peer, col))
-
-    def start_out(k, carry):
-        out_copy(lax.rem(me + k, experts)).start()
-        return carry
-
-    lax.fori_loop(1, experts, start_out, 0)
-    mine = pltpu.make_async_copy(piece(me), landing(me, me), local_sem.at[1])
-    mine.start()
-
-    gain = gain_ref[...]
-    rstd = column_of(rstd_ref[...], rows)
-    swished_grad = lax.dot_general(
-        whole[...], proj_ref[...], OUTER_DIMS, preferred_element_type=jnp.float32
-    )
-    normed = (conv_out_ref[...].astype(jnp.float32) - column_of(mean_ref[...], rows)) * rstd
-    scaled = normed * gain
-    sig = jax.nn.sigmoid(scaled)
-    scaled_grad = swished_grad * sig * (1.0 + scaled * (1.0 - sig)) * gain
-    grads[...] = scaled_grad
-    norms[...] = normed
-    first = jnp.sum(scaled_grad, axis=1, keepdims=True)
-    second = jnp.sum(scaled_grad * normed, axis=1, keepdims=True)
-    lane = lax.broadcasted_iota(jnp.int32, (rows, 128), 1)
-    both = jnp.where(lane == 0, first, second)
-    stats[parts] = both.T[:8]
-    stat_copies = []
-    for k in range(1, parts):
-        copy = remote(
-            stats.at[parts], stats.at[k], stat_send.at[k], stat_recv.at[k],
-            (me, lax.rem(col + k, parts)),
-        )
-        copy.start()
-        stat_copies.append(copy)
-    for copy in stat_copies:
-        copy.wait()
-    total = stats[parts]
-    for k in range(1, parts):
-        total = total + stats[k]
-    total = total / full
-    spread = jnp.concatenate([total] * 16, axis=0).T
-    first_mean = spread[:, 0:1]
-    second_mean = spread[:, 1:2]
-    extended[0:rows, :] = rstd * (grads[...] - first_mean - norms[...] * second_mean)
-
-    def halo_copy(device):
-        return remote(
-            extended.at[pl.ds(0, halo), :], extended.at[pl.ds(rows, halo), :],
-            halo_sem.at[0], halo_sem.at[1], (device, col),
-        )
-
-    @pl.when(me > 0)
-    def _():
-        halo_copy(lax.rem(me + experts - 1, experts)).start()
-
-    @pl.when(me == experts - 1)
-    def _():
-        extended[rows:, :] = jnp.zeros((halo, width), jnp.float32)
-
-    @pl.when(me < experts - 1)
-    def _():
-        halo_copy(lax.rem(me + experts - 1, experts)).wait_recv()
-
-    for start in range(0, width, 128):
-        cols = pl.ds(start, 128)
-        total = jnp.zeros((rows, 128), jnp.float32)
-        for offset in range(tap_count):
-            total = total + taps_ref[offset : offset + 1, cols] * extended[pl.ds(offset, rows), cols]
-        conv_ref[:, cols] = total.astype(jnp.bfloat16)
-
-    def finish(k, carry):
-        source = lax.rem(me - k + experts, experts)
-        remote(
-            piece(source), landing(me, source), out_send.at[source], out_recv.at[source], (source, col)
-        ).wait_recv()
-        out_copy(source).wait_send()
-        return carry
-
-    lax.fori_loop(1, experts, finish, 0)
-    mine.wait()
-    half = experts // 2 * rows
-    proj_grad_ref[...] = jnp.dot(
-        arrived[:, :half], near_ref[...].reshape(half, width), preferred_element_type=jnp.float32
-    )
-    far_copy.wait()
-    proj_grad_ref[...] += jnp.dot(
-        arrived[:, half:], far[...].reshape(half, width), preferred_element_type=jnp.float32
-    )
-    for copy in copies:
-        copy.wait_send()
-
-    @pl.when(me > 0)
-    def _():
-        halo_copy(lax.rem(me + experts - 1, experts)).wait_send()
-
-
-def tail(stream_t, conv_out, mean, rstd, gain, taps, proj, near, experts, parts):
-    width, rows = stream_t.shape
-    full = width * parts
-    block = full // experts
-    halo = -(-(taps.shape[0] - 1) // 8) * 8
-    return pl.pallas_call(
-        functools.partial(tail_kernel, experts, parts),
-        out_shape=(
-            jax.ShapeDtypeStruct((rows, width), jnp.bfloat16),
-            jax.ShapeDtypeStruct((block, width), jnp.float32),
-        ),
-        in_specs=[pl.BlockSpec(memory_space=VMEM)] * 8,
-        out_specs=[pl.BlockSpec(memory_space=VMEM)] * 2,
-        scratch_shapes=[
-            VMEM((full, rows), jnp.bfloat16),
-            VMEM((block, experts * rows), jnp.bfloat16),
-            VMEM(near.shape, jnp.bfloat16),
-            VMEM((rows + halo, width), jnp.float32),
-            VMEM((parts + 1, 8, rows), jnp.float32),
-            VMEM((rows, width), jnp.float32),
-            VMEM((rows, width), jnp.float32),
-            pltpu.SemaphoreType.DMA((parts - 1,)),
-            pltpu.SemaphoreType.DMA((parts - 1,)),
-            pltpu.SemaphoreType.DMA((experts,)),
-            pltpu.SemaphoreType.DMA((experts,)),
-            pltpu.SemaphoreType.DMA((parts,)),
-            pltpu.SemaphoreType.DMA((parts,)),
-            pltpu.SemaphoreType.DMA((2,)),
-            pltpu.SemaphoreType.DMA((2,)),
-            pltpu.SemaphoreType.DMA((2,)),
-        ],
-        compiler_params=pltpu.CompilerParams(
-            collective_id=2, has_side_effects=True, vmem_limit_bytes=67_000_000
-        ),
-        name="tail",
-    )(stream_t, conv_out, mean, rstd, gain, taps, proj, near)
-
-
 def body(
     out_cotangent,
     expert_input,
@@ -701,35 +819,10 @@
     taps,
     out_proj,
 ):
-    tok_rows = out_cotangent.shape[0]
-    experts = lax.axis_size("sp")
-    parts = lax.axis_size("tp")
-    capacity = -(-3 * tok_rows // (experts * 16)) * 16
-    slots = experts * capacity
-
-    chosen = routes[:, :, None] == jnp.arange(experts, dtype=jnp.int32)[None, None, :]
-    named = jnp.any(chosen, axis=1)
-    weight = jnp.sum(jnp.where(chosen, route_weights[:, :, None], 0.0), axis=1)
-    before = jnp.arange(tok_rows)[None, :] < jnp.arange(tok_rows)[:, None]
-    rank = jnp.dot(
-        before.astype(jnp.bfloat16), named.astype(jnp.bfloat16), preferred_element_type=jnp.float32
-    ).astype(jnp.int32)
-    rank = jnp.where(named, rank, -1)
-    pick = rank.T[:, None, :] == jnp.arange(capacity, dtype=jnp.int32)[None, :, None]
-    slot_weight = jnp.sum(jnp.where(pick, weight.T[:, None, :], 0.0), axis=2)
-    pick = pick.astype(jnp.bfloat16).reshape(slots, tok_rows)
-    send_rows = jnp.dot(pick, expert_input, preferred_element_type=jnp.float32).astype(jnp.bfloat16)
-    send_cot = (
-        jnp.dot(pick, out_cotangent, preferred_element_type=jnp.float32)
-        * slot_weight.reshape(slots, 1)
-    ).astype(jnp.bfloat16)
-    mean, rstd, gain = conv_mean[None, :], conv_rstd[None, :], norm_gain[None, :]
-    rows, cot, act, gate_back, up_back, stream, stream_t, near = front(
-        send_rows, send_cot, pick.T, out_cotangent, conv_out, mean, rstd, gain,
-        gate_proj, up_proj, down_proj, experts, parts,
-    )
-    conv_in_grad, proj_grad = tail(
-        stream_t, conv_out, mean, rstd, gain, taps, out_proj, near, experts, parts
+    rows, cot, act, gate_back, up_back, stream, conv_in_grad, proj_grad = step(
+        expert_input, out_cotangent, routes.T, route_weights.T, conv_out, conv_mean[None, :],
+        conv_rstd[None, :], norm_gain[None, :], taps, gate_proj, up_proj, down_proj, out_proj,
+        lax.axis_size("sp"), lax.axis_size("tp"),
     )
     gate_grad, up_grad, down_grad = grads(rows, cot, act, gate_back, up_back)
     return (gate_grad, up_grad, down_grad, proj_grad, stream, conv_in_grad)

time: 106 us -> 87.9 us (0.83)
  Pallas kernels: 96.6 us -> 85 us
  matrix products: 4.07 us -> 0 us
  other arithmetic: 2.22 us -> 0 us
    pallas_call x2 -> x1, Pallas kernels: 87 us -> 75.4 us  [step(): pl.pallas_call(functools.partial(step_kernel, experts, parts), out_shape=...]
    dot_general x3 -> x0, matrix products: 4.07 us -> none  [the longest x1 1.97 us: body(): jnp.dot(pick, out_cotangent, preferred_element_type=jnp.float32)]
where the time goes in v4:
time: 87.9 us; the launch traced here: 87.8 us
  Pallas kernels  85 us (97%)
  local copies, waits for them, and re-layouts  2.12 us (2%)
    pallas_call x1, Pallas kernels, step(): pl.pallas_call(functools.partial(step_kernel, experts, parts), out_shape=...  75.4 us
    pallas_call x1, Pallas kernels, grads(): pl.pallas_call(grads_kernel, grid=(parts,), out_shape=(tall, tall, jax.Sh...  9.61 us
    unnamed x9, local copies, waits for them, and re-layouts  2.12 us

profile of v4, /device:TPU:0, one launch (start us, length us, event | category | flops | bytes accessed | tf_op | source)
XLA Modules:
  0.0 87.8 jit_solution(5969296511572955071)
XLA Ops:
  0.6 75.4 %step.1 = (bf16[4,384,512]{2,1,0:T(8,128)(2,1)}, bf16[4,384,512]{2,1,0:T(8,128)(2,1)}, bf16[384,896]{1,0:T(8,128)(2,1)}, bf16[384,896]{1,0:T(8,128)(2,1)}, bf16[...) custom-call(bf16[128,512]{1,0:T(8,128)(2,1)} %tokens_ref.1, ...), custom_call_target="tpu_custom_call" | custom-call | tf_op jit(solution)/shard_map/step/pallas_call | solution.py:698
  76.0 0.0 copy-start
  76.1 0.0 copy-start.2
  76.1 0.0 copy-start.1
  76.1 9.6 %grads.1 = (bf16[1,2048,896]{2,1,0:T(8,128)(2,1)}, bf16[1,2048,896]{2,1,0:T(8,128)(2,1)}, bf16[1,896,2048]{2,1,0:T(8,128)(2,1)}) custom-call(bf16[4,384,512]{2,1,0:T(8,128)(2,1)} %get-tuple-element.17.rows_ref, bf16[4,384,512]{2,1,0:T(8,128)(2,1)} %get-tuple-element.18.cot_ref, bf16[384,896]{1,0:T(8,128)(2,1)} %get-tuple-element.19.act_ref, ...), custom_call_target="tpu_custom_call" | custom-call | tf_op jit(solution)/shard_map/grads/pallas_call | solution.py:797
  85.7 0.0 copy-done
  85.7 0.8 copy.22
  86.5 0.0 copy-done.2
  86.5 0.7 copy.23
  87.1 0.0 copy-done.1
  87.1 0.7 copy.24
Async XLA Ops:
  76.0 9.6 %copy-start = (f32[256,512]{1,0:T(8,128)S(1)}, f32[256,512]{1,0:T(8,128)}, u32[]{:S(2)}) copy-start(f32[256,512]{1,0:T(8,128)} %get-tuple-element.37) | copy-start | bytes 1572868
  76.1 10.4 %copy-start.2 = (bf16[128,512]{1,0:T(8,128)(2,1)S(1)}, bf16[128,512]{1,0:T(8,128)(2,1)}, u32[]{:S(2)}) copy-start(bf16[128,512]{1,0:T(8,128)(2,1)} %get-tuple-element.38) | copy-start | bytes 393220
  76.1 11.1 %copy-start.1 = (bf16[128,512]{1,0:T(8,128)(2,1)S(1)}, bf16[128,512]{1,0:T(8,128)(2,1)}, u32[]{:S(2)}) copy-start(bf16[128,512]{1,0:T(8,128)(2,1)} %get-tuple-element.39) | copy-start | bytes 393220

commit v5 on v4

--- a/solution.py
+++ b/solution.py
@@ -113,12 +113,6 @@
     rows_send_ref[...] = jnp.dot(
         pick[...], tokens_ref[...], preferred_element_type=jnp.float32
     ).astype(jnp.bfloat16)
-    for expert in range(experts):
-        mine = pl.ds(expert * capacity, capacity)
-        cot_send_ref[mine, :] = (
-            jnp.dot(pick[mine, :], cotangent_ref[...], preferred_element_type=jnp.float32)
-            * slot_weights[expert]
-        ).astype(jnp.bfloat16)
     gather_hails(len(peers))
     sends = (rows_send_ref, cot_send_ref)
 
@@ -180,12 +174,25 @@
             for slot in range(len(held[levels - 1])):
                 hop_arrival(kind, levels - 1, slot, source).wait_recv()
 
-    for kind in range(2):
-        first_hops(kind, me, True)
-    for kind in range(2):
-        for mask in range(1, experts):
-            peer = masked(me, mask)
-            out_copy(kind, peer, me).start()
+    half = experts // 2
+    near, far = list(range(half)), list(range(half, experts))
+
+    def leave(kind, masks):
+        for mask in masks:
+            out_copy(kind, masked(me, mask), me).start()
+
+    first_hops(0, me, True)
+    leave(0, near[1:])
+    for expert in range(experts):
+        mine = pl.ds(expert * capacity, capacity)
+        cot_send_ref[mine, :] = (
+            jnp.dot(pick[mine, :], cotangent_ref[...], preferred_element_type=jnp.float32)
+            * slot_weights[expert]
+        ).astype(jnp.bfloat16)
+    first_hops(1, me, True)
+    leave(1, near[1:])
+    leave(0, far)
+    leave(1, far)
     own = []
     for kind in range(2):
         own.append(
@@ -243,15 +250,12 @@
     def sw_arrive(level):
         for slot, source in enumerate(sources[level]):
             sw_copy(level, slot, flipped(source, far_bits[level])).wait_recv()
-            side_copy(flipped(source, far_bits[level])).start()
 
     def sw_pass():
         sw_arrive(0)
         if len(far_bits) > 1:
             sw_start(1)
 
-    half = experts // 2
-    near, far = list(range(half)), list(range(half, experts))
     own_half = me // half
     span = half * capacity
 
@@ -262,10 +266,11 @@
     def joined(kind, rows):
         return jnp.concatenate([full[kind, part, rows, :] for part in range(parts)], axis=1)
 
-    def pre(cols):
-        rows = joined(0, slice(None))
-        gate_pre[:, cols] = jnp.dot(rows, gate[:, cols], preferred_element_type=jnp.float32)
-        up_pre[:, cols] = jnp.dot(rows, up[:, cols], preferred_element_type=jnp.float32)
+    def pre(side, cols):
+        at = half_rows(side)
+        rows = joined(0, at)
+        gate_pre[at, cols] = jnp.dot(rows, gate[:, cols], preferred_element_type=jnp.float32)
+        up_pre[at, cols] = jnp.dot(rows, up[:, cols], preferred_element_type=jnp.float32)
 
     def back_tile(side, cols, size):
         act_grad[:, 0:size] = lax.dot_general(
@@ -297,29 +302,10 @@
         if hidden % 256:
             back_tile(side, pl.ds(hidden - hidden % 256, hidden % 256), hidden % 256)
 
-    arrive(0, range(1, experts))
-    arrive(1, near[1:])
-    pass_on(0, range(experts))
-    collect(0, range(experts))
-    loads[0].wait()
-    loads[1].wait()
-    tile_starts = list(range(0, hidden, 256))
-    waiting = list(far)
-    for index, start in enumerate(tile_starts):
-        upto = len(far) * (index + 1) // len(tile_starts)
-        arrive(1, far[len(far) - len(waiting) : upto])
-        waiting = far[upto:]
-        pre(pl.ds(start, min(256, hidden - start)))
-    sw_start(0)
-    pass_on(1, near)
-    collect(1, near)
-    loads[2].wait()
-    back(0)
-
     kept = [[col]]
     for bit in bits:
         kept.insert(0, kept[0] + [flipped(column, bit) for column in kept[0]])
-    order = near[1:] + far + [0]
+    order = far + near[1:] + [0]
 
     def first_copy(slot, side):
         rows = half_rows(side)
@@ -377,10 +363,58 @@
                 work[back_starts[1] + slot - size, block_rows(block), :] = summed(1, slot, block)
                 back_copy(1, slot - size, block).start()
 
-    fill_sent(0)
+    def fill_kept(side):
+        for slot in reversed(range(size)):
+            fill(flipped(kept[1][slot], up_bits[0]), side)
+            first_copy(slot, side).start()
+
+    def fill_own(side):
+        for slot in reversed(range(size)):
+            fill(kept[1][slot], side)
+
+    tile_starts = list(range(0, hidden, 256))
+
+    def pre_near(start):
+        pre(0, pl.ds(start, min(256, hidden - start)))
+
+    def back_near(start):
+        if start == 0:
+            collect(1, near)
+            loads[2].wait()
+        size = min(256, hidden - start)
+        back_tile(0, pl.ds(start, size), size)
+
+    arrive(0, near[1:])
+    arrive(1, near[1:])
+    events = [(0, mask) for mask in far] + [(1, mask) for mask in far]
+    ahead = len(far) // 2
+    arrive(0, far[:ahead])
+    pass_on(0, near)
+    pass_on(1, near)
+    collect(0, near)
+    loads[0].wait()
+    loads[1].wait()
+    steps = [functools.partial(pre_near, start) for start in tile_starts]
+    steps += [functools.partial(back_near, start) for start in tile_starts]
+    steps += [functools.partial(fill_sent, 0), functools.partial(fill_kept, 0)]
+    steps += [functools.partial(fill_own, 0)]
+    done = 0
+    events = events[ahead:]
+    for index, (kind, mask) in enumerate(events):
+        arrive(kind, [mask])
+        upto = len(steps) * (index + 1) // len(events)
+        for task in steps[done:upto]:
+            task()
+        done = upto
+    sw_start(0)
+    pass_on(0, far)
+    send_sums(0)
+    collect(0, far)
+    for start in tile_starts:
+        pre(1, pl.ds(start, min(256, hidden - start)))
     pass_on(1, far)
-    send_sums(0)
     collect(1, far)
+    sw_pass()
     back(1)
     saves = [
         pltpu.make_async_copy(full.at[0], rows_out, save_sem.at[0]),
@@ -390,15 +424,11 @@
         pltpu.make_async_copy(backs.at[2], up_out, save_sem.at[4]),
     ]
     fill_sent(1)
-    sw_pass()
+    fill_kept(1)
     send_sums(1)
+    fill_own(1)
     for copy in saves:
         copy.start()
-    for slot in reversed(range(size)):
-        fill(flipped(kept[1][slot], up_bits[0]), None)
-        for side in range(2):
-            first_copy(slot, side).start()
-        fill(kept[1][slot], None)
     for slot in range(size):
         for side in range(2):
             first_copy(slot, side).wait_recv()
@@ -434,6 +464,8 @@
         sw_arrive(level)
         if level + 1 < len(far_bits):
             sw_start(level + 1)
+    for source in sources[-1][1:]:
+        side_copy(source).start()
     for mask in order[:-1]:
         source = masked(me, mask)
         home_copy(source, source).wait_recv()
@@ -774,34 +806,53 @@
     )
 
 
-def grads_kernel(rows_ref, cot_ref, act_ref, gate_ref, up_ref, gate_out, up_out, down_out):
-    rows = rows_ref[...]
-    gate_out[...] = lax.dot_general(
-        rows, gate_ref[...], OUTER_DIMS, preferred_element_type=jnp.float32
+def grads_kernel(
+    rows_ref, cot_ref, act_ref, gate_ref, up_ref, stream_ref, conv_ref, proj_ref,
+    gate_out, up_out, down_out, stream_out, conv_out, proj_out, act_t,
+):
+    stream_out[...] = stream_ref[...]
+    conv_out[...] = conv_ref[...]
+    proj_out[...] = proj_ref[...]
+
+    @pl.when(pl.program_id(0) == 0)
+    def _():
+        act_t[...] = act_ref[...].T
+
+    rows_t = rows_ref[...].T
+    gate_out[...] = jnp.dot(
+        rows_t, gate_ref[...], preferred_element_type=jnp.float32
     ).astype(jnp.bfloat16)
-    up_out[...] = lax.dot_general(
-        rows, up_ref[...], OUTER_DIMS, preferred_element_type=jnp.float32
+    up_out[...] = jnp.dot(
+        rows_t, up_ref[...], preferred_element_type=jnp.float32
     ).astype(jnp.bfloat16)
-    down_out[...] = lax.dot_general(
-        act_ref[...], cot_ref[...], OUTER_DIMS, preferred_element_type=jnp.float32
+    down_out[...] = jnp.dot(
+        act_t[...], cot_ref[...], preferred_element_type=jnp.float32
     ).astype(jnp.bfloat16)
 
 
-def grads(rows, cot, act, gate_back, up_back):
+def grads(rows, cot, act, gate_back, up_back, stream, conv, proj):
     parts, slots, width = rows.shape
     hidden = act.shape[1]
     piece = pl.BlockSpec((None, slots, width), lambda i: (i, 0, 0))
     acts = pl.BlockSpec((slots, hidden), lambda i: (0, 0))
     across = pl.BlockSpec((None, width, hidden), lambda i: (0, i, 0))
     tall = jax.ShapeDtypeStruct((1, width * parts, hidden), jnp.bfloat16)
+
+    def strip(array):
+        return pl.BlockSpec((array.shape[0] // parts, array.shape[1]), lambda i: (i, 0))
+
+    passed = (stream, conv, proj)
     return pl.pallas_call(
         grads_kernel,
         grid=(parts,),
-        out_shape=(tall, tall, jax.ShapeDtypeStruct((1, hidden, width * parts), jnp.bfloat16)),
-        in_specs=[piece, piece, acts, acts, acts],
-        out_specs=[across, across, pl.BlockSpec((None, hidden, width), lambda i: (0, 0, i))],
+        out_shape=(tall, tall, jax.ShapeDtypeStruct((1, hidden, width * parts), jnp.bfloat16))
+        + tuple(jax.ShapeDtypeStruct(array.shape, array.dtype) for array in passed),
+        in_specs=[piece, piece, acts, acts, acts] + [strip(array) for array in passed],
+        out_specs=[across, across, pl.BlockSpec((None, hidden, width), lambda i: (0, 0, i))]
+        + [strip(array) for array in passed],
+        scratch_shapes=[VMEM((hidden, slots), jnp.bfloat16)],
         name="grads",
-    )(rows, cot, act, gate_back, up_back)
+    )(rows, cot, act, gate_back, up_back, *passed)
 
 
 def body(
@@ -824,7 +875,9 @@
         conv_rstd[None, :], norm_gain[None, :], taps, gate_proj, up_proj, down_proj, out_proj,
         lax.axis_size("sp"), lax.axis_size("tp"),
     )
-    gate_grad, up_grad, down_grad = grads(rows, cot, act, gate_back, up_back)
+    gate_grad, up_grad, down_grad, stream, conv_in_grad, proj_grad = grads(
+        rows, cot, act, gate_back, up_back, stream, conv_in_grad, proj_grad
+    )
     return (gate_grad, up_grad, down_grad, proj_grad, stream, conv_in_grad)
 
 

time: 87.9 us -> 83.2 us (0.947)
  Pallas kernels: 85 us -> 82.2 us
  local copies, waits for them, and re-layouts: 2.12 us -> 0 us
    pallas_call x1, Pallas kernels: 75.4 us -> 71.9 us  [step(): pl.pallas_call(functools.partial(step_kernel, experts, parts), out_shape=...]
    unnamed x9 -> x0, local copies, waits for them, and re-layouts: 2.12 us -> none
where the time goes in v5:
time: 83.2 us; the launch traced here: 83 us
  Pallas kernels  82.2 us (99%)
    pallas_call x1, Pallas kernels, step(): pl.pallas_call(functools.partial(step_kernel, experts, parts), out_shape=...  71.9 us
    pallas_call x1, Pallas kernels, grads(): pl.pallas_call(grads_kernel, grid=(parts,), out_shape=(tall, tall, jax.Sh...  10.3 us

profile of v5, /device:TPU:0, one launch (start us, length us, event | category | flops | bytes accessed | tf_op | source)
XLA Modules:
  0.0 83.0 jit_solution(6929139328006448859)
XLA Ops:
  0.6 71.9 %step.1 = (bf16[4,384,512]{2,1,0:T(8,128)(2,1)}, bf16[4,384,512]{2,1,0:T(8,128)(2,1)}, bf16[384,896]{1,0:T(8,128)(2,1)}, bf16[384,896]{1,0:T(8,128)(2,1)}, bf16[...) custom-call(bf16[128,512]{1,0:T(8,128)(2,1)} %tokens_ref.1, ...), custom_call_target="tpu_custom_call" | custom-call | tf_op jit(solution)/shard_map/step/pallas_call | solution.py:730
  72.5 10.3 %grads.1 = (bf16[1,2048,896]{2,1,0:T(8,128)(2,1)}, bf16[1,2048,896]{2,1,0:T(8,128)(2,1)}, bf16[1,896,2048]{2,1,0:T(8,128)(2,1)}, bf16[128,512]{1,0:T(8,128)(2,1)...) custom-call(bf16[4,384,512]{2,1,0:T(8,128)(2,1)} %get-tuple-element.20.rows_ref, ...), custom_call_target="tpu_custom_call" | custom-call | tf_op jit(solution)/shard_map/grads/pallas_call | solution.py:845

commit v6 on v5

--- a/solution.py
+++ b/solution.py
@@ -273,34 +273,22 @@
         up_pre[at, cols] = jnp.dot(rows, up[:, cols], preferred_element_type=jnp.float32)
 
     def back_tile(side, cols, size):
-        act_grad[:, 0:size] = lax.dot_general(
+        grad = lax.dot_general(
             joined(1, half_rows(side)), down[cols, :], INNER_DIMS,
             preferred_element_type=jnp.float32,
         )
-        base = (own_half if side == 0 else 1 - own_half) * half
-
-        def chunk(k, carry):
-            rows = block_rows(base + k)
-            gates, ups, grad = gate_pre[rows, cols], up_pre[rows, cols], act_grad[block_rows(k), 0:size]
-            sig = jax.nn.sigmoid(gates)
-            silu = gates * sig
-            backs[0, rows, cols] = (silu * ups).astype(jnp.bfloat16)
-            backs[1, rows, cols] = (grad * ups * sig * (1.0 + gates * (1.0 - sig))).astype(
-                jnp.bfloat16
-            )
-            backs[2, rows, cols] = (grad * silu).astype(jnp.bfloat16)
-            return carry
-
-        lax.fori_loop(0, half, chunk, 0)
+        at = half_rows(side)
+        gates, ups = gate_pre[at, cols], up_pre[at, cols]
+        sig = jax.nn.sigmoid(gates)
+        silu = gates * sig
+        backs[0, at, cols] = (silu * ups).astype(jnp.bfloat16)
+        backs[1, at, cols] = (grad * ups * sig * (1.0 + gates * (1.0 - sig))).astype(jnp.bfloat16)
+        backs[2, at, cols] = (grad * silu).astype(jnp.bfloat16)
 
     def back(side):
-        def one(j, carry):
-            back_tile(side, pl.ds(pl.multiple_of(j * 256, 256), 256), 256)
-            return carry
-
-        lax.fori_loop(0, hidden // 256, one, 0)
-        if hidden % 256:
-            back_tile(side, pl.ds(hidden - hidden % 256, hidden % 256), hidden % 256)
+        for start in range(0, hidden, 256):
+            size = min(256, hidden - start)
+            back_tile(side, pl.ds(start, size), size)
 
     kept = [[col]]
     for bit in bits:
@@ -387,7 +375,7 @@
     arrive(0, near[1:])
     arrive(1, near[1:])
     events = [(0, mask) for mask in far] + [(1, mask) for mask in far]
-    ahead = len(far) // 2
+    ahead = 3 * len(far) // 4
     arrive(0, far[:ahead])
     pass_on(0, near)
     pass_on(1, near)

time: 83.2 us -> 79.4 us (0.954)
  Pallas kernels: 82.2 us -> 78.4 us
    pallas_call x1, Pallas kernels: 71.9 us -> 68 us  [step(): pl.pallas_call(functools.partial(step_kernel, experts, parts), out_shape=...]
where the time goes in v6:
time: 79.4 us; the launch traced here: 79.2 us
  Pallas kernels  78.4 us (99%)
  between operations  0.8 us (1%)
    pallas_call x1, Pallas kernels, step(): pl.pallas_call(functools.partial(step_kernel, experts, parts), out_shape=...  68 us
    pallas_call x1, Pallas kernels, grads(): pl.pallas_call(grads_kernel, grid=(parts,), out_shape=(tall, tall, jax.Sh...  10.3 us

profile of v6, /device:TPU:0, one launch (start us, length us, event | category | flops | bytes accessed | tf_op | source)
XLA Modules:
  0.0 79.2 jit_solution(10000273768323988387)
XLA Ops:
  0.6 68.0 %step.1 = (bf16[4,384,512]{2,1,0:T(8,128)(2,1)}, bf16[4,384,512]{2,1,0:T(8,128)(2,1)}, bf16[384,896]{1,0:T(8,128)(2,1)}, bf16[384,896]{1,0:T(8,128)(2,1)}, bf16[...) custom-call(bf16[128,512]{1,0:T(8,128)(2,1)} %tokens_ref.1, ...), custom_call_target="tpu_custom_call" | custom-call | tf_op jit(solution)/shard_map/step/pallas_call | solution.py:718
  68.7 10.3 %grads.1 = (bf16[1,2048,896]{2,1,0:T(8,128)(2,1)}, bf16[1,2048,896]{2,1,0:T(8,128)(2,1)}, bf16[1,896,2048]{2,1,0:T(8,128)(2,1)}, bf16[128,512]{1,0:T(8,128)(2,1)...) custom-call(bf16[4,384,512]{2,1,0:T(8,128)(2,1)} %get-tuple-element.20.rows_ref, ...), custom_call_target="tpu_custom_call" | custom-call | tf_op jit(solution)/shard_map/grads/pallas_call | solution.py:833
